TPU v7x, 512 devices: a whole 4x4x16 slice. The times are simulated.
512 devices in a mesh: ra: 16 (over y, x), cb: 32 (over z, core).
Axes of the slice: x: 4, y: 4, z: 16, core: 2. Of those that a mesh axis runs over, the one named last changes fastest.
Arguments:
- tokens: bfloat16 [8192, 2048], P('cb', 'ra'), may hold values from -40 to 40
- gain_first: float32 [2048], replicated, may hold values from 0.1 to 1.9
- gate_first: float32 [2048, 5632], P('cb', 'ra'), may hold values from -0.125 to 0.125
- gate_first_scale: float32 [5632], P('ra'), may hold values from 0.5 to 2
- up_first: float32 [2048, 5632], P('cb', 'ra'), may hold values from -0.125 to 0.125
- up_first_scale: float32 [5632], P('ra'), may hold values from 0.5 to 2
- down_first: float32 [5632, 2048], P('ra', 'cb'), may hold values from -0.078125 to 0.078125
- down_first_scale: float32 [2048], replicated, may hold values from 0.5 to 2
- gain_second: float32 [2048], replicated, may hold values from 0.1 to 1.9
- gate_second: float32 [2048, 5632], P('cb', 'ra'), may hold values from -0.125 to 0.125
- gate_second_scale: float32 [5632], P('ra'), may hold values from 0.5 to 2
- up_second: float32 [2048, 5632], P('cb', 'ra'), may hold values from -0.125 to 0.125
- up_second_scale: float32 [5632], P('ra'), may hold values from 0.5 to 2
- down_second: float32 [5632, 2048], P('ra', 'cb'), may hold values from -0.078125 to 0.078125
- down_second_scale: float32 [2048], replicated, may hold values from 0.5 to 2
- gain_last: float32 [2048], replicated, may hold values from 0.1 to 1.9
Outputs:
- mixed: bfloat16 [8192, 2048], P('cb', 'ra')
All inputs are finite; a program needn't handle non-finite values.
Results may differ from a plain program's by a relative error of at most 0.025.
Values may be sent and summed in bfloat16 or wider, within the bound.
No kernel may reach another device: no remote copies, remote signals or barrier semaphores. Data moves between devices by JAX's collectives and lax.ppermute only.
A program may use at most 64 MiB of HBM per device.

v0:
```python
import functools

import jax
import jax.numpy as jnp
from jax import lax
from jax.experimental import pallas as pl
from jax.experimental.pallas import tpu as pltpu
from jax.sharding import Mesh
from jax.sharding import PartitionSpec as P


D = 2048
HALF = D // 2
RA = ("ra_0", "ra_1")
CB = ("cb_0", "cb_1")
TILE = 128
TILES = 17
PART = 9
WIDE = 4 * TILE
EPS = 1e-06
LIFT = 2.0**18
ROOM = pltpu.CompilerParams(vmem_limit_bytes=20 * 1024 * 1024)
MOST = pltpu.CompilerParams(vmem_limit_bytes=24 * 1024 * 1024)
VMEM = pl.BlockSpec(memory_space=pltpu.VMEM)
HBM = pl.BlockSpec(memory_space=pltpu.HBM)


def pack_body(*refs):
    pieces, tokens, out, copies, held, wide, own, sems, copy_sems = refs[:6], *refs[6:]
    loads = [pltpu.make_async_copy(p, held.at[j], sems.at[j]) for j, p in enumerate(pieces)]
    token_load = pltpu.make_async_copy(tokens, own, sems.at[len(pieces)])
    sends = [
        pltpu.make_async_copy(own, copies.at[j], copy_sems.at[j]) for j in range(copies.shape[0])
    ]
    token_load.start()
    for load in loads:
        load.start()
    token_load.wait()
    for send in sends:
        send.start()
    rows, width = held.shape[1:]
    wide[...] = jnp.zeros_like(wide)
    tiles = [None] * TILES
    for j, load in enumerate(loads):
        load.wait()
        wide[:, :width] = held[j]
        first, shift = divmod(j * width, TILE)
        turned = pltpu.roll(wide[...], shift, axis=1) if shift else wide[...]
        for k in range(-(-(width + shift) // TILE)):
            part = turned[:, k * TILE : (k + 1) * TILE]
            old = tiles[first + k]
            tiles[first + k] = part if old is None else old + part
    for j, tile in enumerate(tiles):
        out[j * rows : (j + 1) * rows] = tile.astype(jnp.bfloat16) * LIFT
    for send in sends:
        send.wait()


def pack(tokens, *pieces):
    rows, width = pieces[0].shape
    count = lax.axis_size(RA)
    return pl.pallas_call(
        pack_body,
        in_specs=[HBM] * 7,
        out_specs=[VMEM, HBM],
        out_shape=(
            jax.ShapeDtypeStruct((TILES * rows, TILE), jnp.bfloat16),
            jax.ShapeDtypeStruct((count, *tokens.shape), tokens.dtype),
        ),
        scratch_shapes=[
            pltpu.VMEM((6, rows, width), jnp.float32),
            pltpu.VMEM((rows, WIDE), jnp.float32),
            pltpu.VMEM(tokens.shape, tokens.dtype),
            pltpu.SemaphoreType.DMA((7,)),
            pltpu.SemaphoreType.DMA((count,)),
        ],
    )(*pieces, tokens)


def halves(left, right):
    low = lax.broadcasted_iota(jnp.int32, left.shape, 1) < TILE // 2
    turn = functools.partial(pltpu.roll, shift=TILE // 2, axis=1)
    return jnp.where(low, left, turn(right)), jnp.where(low, turn(left), right)


def to_split(tiles):
    pairs = [halves(*tiles[j : j + 2]) for j in range(0, len(tiles), 2)]
    return [a for a, _ in pairs] + [b for _, b in pairs]


def from_split(tiles):
    count = len(tiles) // 2
    pairs = [halves(tiles[j], tiles[j + count]) for j in range(count)]
    return [tile for pair in pairs for tile in pair]


def tiles_of(value):
    return [value[:, j : j + TILE] for j in range(0, value.shape[1], TILE)]


def split_row(vector):
    rows = jnp.broadcast_to(vector[...], (8, D))
    return jnp.concatenate(to_split(tiles_of(rows)), axis=1)[:1]


def spread_body(pieces, gain, out, own):
    count, rows, _ = pieces.shape
    total = jnp.zeros((rows, 1), jnp.float32)
    for j in range(count):
        piece = pieces[j].astype(jnp.float32)
        total += jnp.sum(piece * piece, axis=1, keepdims=True)
    scale = lax.rsqrt(total / D + EPS)
    few = own.shape[0]
    start = pl.multiple_of(lax.axis_index(RA) * few, few)
    for j in range(0, count, 2):
        normed, kept = [], []
        for i in (j, j + 1):
            value = pieces[i].astype(jnp.float32)
            normed.append(value * scale * gain[:, i * TILE : (i + 1) * TILE])
            kept.append(pieces[i, pl.ds(start, few), :].astype(jnp.float32))
        for side in (0, 1):
            at = slice(side * HALF + j // 2 * TILE, side * HALF + (j // 2 + 1) * TILE)
            out[:, at] = halves(*normed)[side].astype(jnp.bfloat16)
            own[:, at] = halves(*kept)[side]


def spread(pieces, gain):
    count, rows, _ = pieces.shape
    return pl.pallas_call(
        spread_body,
        out_shape=(
            jax.ShapeDtypeStruct((rows, D), jnp.bfloat16),
            jax.ShapeDtypeStruct((rows // count, D), jnp.float32),
        ),
        compiler_params=ROOM,
    )(pieces, gain[None])


def block_body(start, x, near, far, s_gate, s_up, out, held, scales, sems):
    rows = near.shape[1] // PART
    loads = [
        [
            pltpu.make_async_copy(
                weights.at[:, pl.ds(j * rows, rows)],
                held.at[side, :, :, pl.ds(j * TILE, TILE)],
                sems.at[side, j],
            )
            for side, weights in enumerate((near, far))
        ]
        for j in range(PART)
    ]
    for pair in loads:
        for load in pair:
            load.start()
    width = s_gate.shape[1]
    scales[...] = jnp.zeros_like(scales)
    scales[0:1, :width] = s_gate[...] / LIFT
    scales[1:2, :width] = s_up[...] / LIFT
    down = (start + 2 * width) // TILE * TILE
    place = start + 2 * width - down
    placed = pltpu.roll(scales[...], place, axis=1)
    core = lax.axis_index("cb_1")
    columns = [
        pl.ds(pl.multiple_of(core * HALF, HALF), HALF),
        pl.ds(pl.multiple_of((1 - core) * HALF, HALF), HALF),
    ]
    across = -(-(start + 2 * width) // TILE)
    both = jnp.zeros((x.shape[0], across * TILE), jnp.float32)
    for side in (0, 1):
        for j in range(across):
            loads[j][side].wait()
        part = held[side, :, :, : across * TILE].reshape(HALF, across * TILE)
        both += jnp.dot(x[:, columns[side]], part, preferred_element_type=jnp.float32)

    def turned(at):
        return pltpu.roll(both, (place - at) % both.shape[1], axis=1)[:, :WIDE]

    gate = turned(start) * placed[0:1]
    upper = turned(start + width) * placed[1:2]
    hidden = (gate / (1.0 + jnp.exp(-gate)) * upper).astype(jnp.bfloat16)
    for side in (0, 1):
        for j in range(across, PART):
            loads[j][side].wait()
        out[:, columns[side]] = lax.dot_general(
            hidden,
            held[side, :, :, down : down + WIDE].reshape(HALF, WIDE),
            (((1,), (1,)), ((), ())),
            preferred_element_type=jnp.float32,
        ).astype(jnp.bfloat16)


def block(x, near, far, start, s_gate, s_up):
    groups, rows = near.shape[0], near.shape[1] // PART
    return pl.pallas_call(
        functools.partial(block_body, start),
        in_specs=[VMEM, HBM, HBM, VMEM, VMEM],
        out_shape=jax.ShapeDtypeStruct(x.shape, jnp.bfloat16),
        scratch_shapes=[
            pltpu.VMEM((2, groups, rows, PART * TILE), jnp.bfloat16),
            pltpu.VMEM((8, WIDE), jnp.float32),
            pltpu.SemaphoreType.DMA((2, PART)),
        ],
        compiler_params=MOST,
    )(x, near, far, s_gate[None], s_up[None])


def join_body(last, pieces, before, scale, gain, *outs):
    count = pieces.shape[0]
    added = pieces[0].astype(jnp.float32)
    for j in range(1, count):
        added += pieces[j].astype(jnp.float32)
    values = 0.1 * before[...] + (0.5 / LIFT) * added * split_row(scale)
    meansq = jnp.sum(values * values, axis=1, keepdims=True) / D
    normed = values * lax.rsqrt(meansq + EPS) * split_row(gain)
    if last:
        (out,) = outs
        for j, tile in enumerate(from_split(tiles_of(normed))):
            out[j] = tile.astype(jnp.bfloat16)
    else:
        out, total = outs
        total[...] = values
        for j in range(count):
            out[j] = normed.astype(jnp.bfloat16)


def join(pieces, before, scale, gain, last):
    count, rows, _ = pieces.shape
    shapes = [jax.ShapeDtypeStruct((count, rows, TILE if last else D), jnp.bfloat16)]
    if not last:
        shapes.append(jax.ShapeDtypeStruct((rows, D), jnp.float32))
    return pl.pallas_call(
        functools.partial(join_body, last), out_shape=shapes, compiler_params=ROOM
    )(pieces, before, scale[None], gain[None])


def exchange(pieces):
    return lax.all_to_all(pieces, RA, split_axis=0, concat_axis=0, tiled=True)


def by_rows(partial_value):
    return exchange(partial_value.reshape(lax.axis_size(RA), -1, D))


def both_cores(weights):
    near = weights.astype(jnp.bfloat16)
    return near, lax.ppermute(near, "cb_1", ((0, 1), (1, 0)))


def shards(
    tokens,
    gain_first,
    gate_first,
    gate_first_scale,
    up_first,
    up_first_scale,
    down_first,
    down_first_scale,
    gain_second,
    gate_second,
    gate_second_scale,
    up_second,
    up_second_scale,
    down_second,
    down_second_scale,
    gain_last,
):
    packed, copies = pack(
        tokens, gate_first, up_first, down_first.T, gate_second, up_second, down_second.T
    )
    pieces = exchange(copies)
    packed = packed.reshape(-1).astype(jnp.float16)
    gathered = lax.all_gather(packed, "cb_0", axis=0, tiled=True)
    rows, width = gate_first.shape
    weights = gathered.reshape(-1, TILES * rows, TILE)
    later, start = divmod(3 * width, TILE)
    near, far = both_cores(weights[:, : PART * rows])
    normed, own = spread(pieces, gain_first)
    partial_first = block(normed, near, far, 0, gate_first_scale, up_first_scale)
    weights, partial_first = lax.optimization_barrier((weights, partial_first))
    near, far = both_cores(weights[:, later * rows :])
    arrived = by_rows(partial_first)
    copies, first = join(arrived, own, down_first_scale, gain_second, False)
    normed = exchange(copies).reshape(-1, D)
    partial_second = block(normed, near, far, start, gate_second_scale, up_second_scale)
    (columns,) = join(by_rows(partial_second), first, down_second_scale, gain_last, True)
    return exchange(columns).reshape(tokens.shape)


def solution(mesh):
    torus = Mesh(mesh.devices.reshape(4, 4, 16, 2), ("ra_0", "ra_1", "cb_0", "cb_1"))
    weight, across = P(CB, RA), P(RA, CB)
    return jax.shard_map(
        shards,
        mesh=torus,
        in_specs=(
            P(CB, RA),
            P(),
            weight,
            P(RA),
            weight,
            P(RA),
            across,
            P(),
            P(),
            weight,
            P(RA),
            weight,
            P(RA),
            across,
            P(),
            P(),
        ),
        out_specs=P(CB, RA),
        check_vma=False,
    )
```

profile of v0, /device:TPU:32, one launch (start us, length us, event | category | flops | bytes accessed | tf_op | source)
XLA Modules:
  0.0 187.2 jit_solution(5095168996198669382)
XLA Ops:
  0.0 2.7 %shard_map.154 = (bf16[1088,128]{1,0:T(8,128)(2,1)}, bf16[16,256,128]{2,1,0:T(8,128)(2,1)}) custom-call(f32[64,352]{1,0:T(8,128)} %refs_0_.1, f32[64,352]{1,0:T(8,128)} %refs_1_.1, f32[64,352]{1,0:T(8,128)} %bitcast.25, f32[64,352]{1,0:T(8,128)} %refs_3_.1, f32[64,352]{1,0:T(8,128)} %refs_4_.1, f32[64,352]{1,0:T(8,128)} %bitcast.26, bf16[256,128]{1,0:T(8,128)(2,1)} %refs_6_.1), custom_call_target="tpu_custom_call" | custom-call | tf_op jit(solution)/shard_map/pallas_call | solution.py:62
  2.7 1.0 convert_bitcast_fusion
  3.7 68.2 %all-gather.1 = f16[2228224]{0:T(1024)(128)(2,1)S(1)} all-gather(f16[139264]{0:T(1024)(128)(2,1)S(1)} %convert_bitcast_fusion), channel_id=1, replica_groups=mesh['ra_0'=4,'ra_1'=4,'cb_0'=16,'cb_1'=2] {'cb_0'}, dimensions={0}, use_global_device_ids=true | all-gather | bytes 4734976 | tf_op jit(solution)/shard_map/all_gather | solution.py:272
  71.9 0.0 copy-start.6
  71.9 0.0 copy-start.8
  71.9 0.0 copy-start.9
  71.9 0.0 copy-start.1
  71.9 0.4 slice_convert_fusion.near
  72.4 1.6 copy-done.6
  73.9 1.9 %collective-permute-start = (bf16[16,576,128]{2,1,0:T(8,128)(2,1)S(1)}, bf16[16,576,128]{2,1,0:T(8,128)(2,1)}, u32[]{:S(2)}, u32[]{:S(2)}) collective-permute-start(bf16[16,576,128]{2,1,0:T(8,128)(2,1)S(1)} %slice_convert_fusion.near), channel_id=1, source_target_pairs={{0,1},{1,0},{2,3},{3,2},{4,5},{5,4},{6,7},{7,6},{8,9},{9,8},{10,11... | collective-permute-start | bytes 7077896 | tf_op jit(solution)/shard_map/ppermute | solution.py:246
  75.9 7.0 %all-to-all-start = ((bf16[16,256,128]{2,1,0:T(8,128)(2,1)}), bf16[16,256,128]{2,1,0:T(8,128)(2,1)S(1)}, u32[]{:S(2)}, u32[]{:S(2)}) async-start(bf16[16,256,128]{2,1,0:T(8,128)(2,1)} %get-tuple-element.14), calls=%async_computation | async-start | bytes 2097152 | tf_op jit(solution)/shard_map/all_to_all | solution.py:237
  82.9 0.0 copy-done.8
  82.9 0.0 copy-done.9
  83.0 18.5 %all-to-all-done.pieces = bf16[16,256,128]{2,1,0:T(8,128)(2,1)S(1)} async-done(((bf16[16,256,128]{2,1,0:T(8,128)(2,1)}), bf16[16,256,128]{2,1,0:T(8,128)(2,1)S(1)}, u32[]{:S(2)}, u32[]{:S(2)}) %all-to-all-start) | async-done | bytes 1048608 | tf_op jit(solution)/shard_map/all_to_all | solution.py:237
  101.5 0.0 copy-done.1
  101.5 1.1 shard_map.155
  102.6 0.0 collective-permute-done.far
  102.6 0.0 copy-start.7
  102.7 4.3 %shard_map.156 = bf16[256,2048]{1,0:T(8,128)(2,1)S(1)} custom-call(bf16[256,2048]{1,0:T(8,128)(2,1)S(1)} %get-tuple-element.15.x, bf16[16,576,128]{2,1,0:T(8,128)(2,1)S(1)} %slice_convert_fusion.near, bf16[16,576,128]{2,1,0:T(8,128)(2,1)} %collective-permute-done.far, f32[1,352]{1,0:T(1,128)S(1)} %broadcast_in_dim.28.s_gate, f32[1,352]{1,0:T(1,128)S(1)} %broadcast_in_dim.29.s_up), custom_call_target="tpu_custom_call" | custom-call | tf_op jit(solution)/shard_map/pallas_call | solution.py:194
  107.0 0.0 copy-done.7
  107.0 0.0 copy-start.2
  107.0 0.0 copy-start.3
  107.0 0.4 slice_convert_fusion.1.near
  107.4 1.9 %collective-permute-start.1 = (bf16[16,576,128]{2,1,0:T(8,128)(2,1)S(1)}, bf16[16,576,128]{2,1,0:T(8,128)(2,1)}, u32[]{:S(2)}, u32[]{:S(2)}) collective-permute-start(bf16[16,576,128]{2,1,0:T(8,128)(2,1)S(1)} %slice_convert_fusion.1.near), channel_id=1, source_target_pairs={{0,1},{1,0},{2,3},{3,2},{4,5},{5,4},{6,7},{7,6},{8,9},{9,8},{10,11... | collective-permute-start | bytes 7077896 | tf_op jit(solution)/shard_map/ppermute | solution.py:246
  109.4 0.0 copy-start.10
  109.4 0.0 copy-start.11
  109.4 20.8 %all_to_all.25.pieces = bf16[16,16,2048]{2,1,0:T(8,128)(2,1)S(1)} all-to-all(bf16[16,16,2048]{2,1,0:T(8,128)(2,1)S(1)} %bitcast.15), channel_id=1, replica_groups=mesh['ra_0'=4,'ra_1'=4,'cb_0'=16,'cb_1'=2] {'ra_0','ra_1'}, dimensions={0} | all-to-all | bytes 2097152 | tf_op jit(solution)/shard_map/all_to_all | solution.py:237
  130.2 0.0 copy-done.2
  130.2 0.0 copy-done.3
  130.2 0.3 shard_map.157
  130.5 0.0 copy-start
  130.5 1.0 copy-done
  131.5 3.7 %all-to-all-start.2 = ((bf16[16,16,2048]{2,1,0:T(8,128)(2,1)}), bf16[16,16,2048]{2,1,0:T(8,128)(2,1)S(1)}, u32[]{:S(2)}, u32[]{:S(2)}) async-start(bf16[16,16,2048]{2,1,0:T(8,128)(2,1)} %copy-done), calls=%async_computation.2 | async-start | bytes 2097152 | tf_op jit(solution)/shard_map/all_to_all | solution.py:237
  135.2 0.0 copy-done.10
  135.2 0.0 copy-done.11
  135.2 17.0 %all-to-all-done.2 = bf16[16,16,2048]{2,1,0:T(8,128)(2,1)S(1)} async-done(((bf16[16,16,2048]{2,1,0:T(8,128)(2,1)}), bf16[16,16,2048]{2,1,0:T(8,128)(2,1)S(1)}, u32[]{:S(2)}, u32[]{:S(2)}) %all-to-all-start.2) | async-done | bytes 1048608 | tf_op jit(solution)/shard_map/all_to_all | solution.py:237
  152.2 0.0 collective-permute-done.1.far
  152.2 0.0 copy-start.4
  152.2 0.0 copy-start.5
  152.2 4.2 %shard_map.158 = bf16[256,2048]{1,0:T(8,128)(2,1)S(1)} custom-call(bf16[256,2048]{1,0:T(8,128)(2,1)S(1)} %bitcast.14, bf16[16,576,128]{2,1,0:T(8,128)(2,1)S(1)} %slice_convert_fusion.1.near, bf16[16,576,128]{2,1,0:T(8,128)(2,1)} %collective-permute-done.1.far, f32[1,352]{1,0:T(1,128)S(1)} %broadcast_in_dim.32.s_gate, f32[1,352]{1,0:T(1,128)S(1)} %broadcast_in_dim.33.s_up), custom_call_target="tpu_custom_call" | custom-call | tf_op jit(solution)/shard_map/pallas_call | solution.py:194
  156.4 19.2 %all_to_all.26.pieces = bf16[16,16,2048]{2,1,0:T(8,128)(2,1)S(1)} all-to-all(bf16[16,16,2048]{2,1,0:T(8,128)(2,1)S(1)} %bitcast.16), channel_id=1, replica_groups=mesh['ra_0'=4,'ra_1'=4,'cb_0'=16,'cb_1'=2] {'ra_0','ra_1'}, dimensions={0} | all-to-all | bytes 2097152 | tf_op jit(solution)/shard_map/all_to_all | solution.py:237
  175.6 0.0 copy-done.4
  175.6 0.0 copy-done.5
  175.6 0.3 shard_map.159
  176.0 10.6 %all_to_all.27 = bf16[16,16,128]{2,1,0:T(8,128)(2,1)S(1)} all-to-all(bf16[16,16,128]{2,1,0:T(8,128)(2,1)S(1)} %shard_map.159), channel_id=1, replica_groups=mesh['ra_0'=4,'ra_1'=4,'cb_0'=16,'cb_1'=2] {'ra_0','ra_1'}, dimensions={0} | all-to-all | bytes 131072 | tf_op jit(solution)/shard_map/all_to_all | solution.py:237
  186.6 0.6 copy.18
  (4 shorter events, 0.0 us)
Async XLA Ops:
  71.9 2.0 %copy-start.6 = (f16[2228224]{0:T(1024)(128)(2,1)}, f16[2228224]{0:T(1024)(128)(2,1)S(1)}, u32[]{:S(2)}) copy-start(f16[2228224]{0:T(1024)(128)(2,1)S(1)} %all-gather.1) | copy-start | bytes 13369348
  71.9 11.0 %copy-start.8 = (f32[352]{0:T(512)S(1)}, f32[352]{0:T(512)}, u32[]{:S(2)}) copy-start(f32[352]{0:T(512)} %param.19) | copy-start | bytes 4228
  71.9 11.0 %copy-start.9 = (f32[352]{0:T(512)S(1)}, f32[352]{0:T(512)}, u32[]{:S(2)}) copy-start(f32[352]{0:T(512)} %param.21) | copy-start | bytes 4228
  71.9 29.6 %copy-start.1 = (f32[2048]{0:T(1024)S(1)}, f32[2048]{0:T(1024)}, u32[]{:S(2)}) copy-start(f32[2048]{0:T(1024)} %param.17) | copy-start | bytes 24580
  73.9 28.7 %collective-permute-start = (bf16[16,576,128]{2,1,0:T(8,128)(2,1)S(1)}, bf16[16,576,128]{2,1,0:T(8,128)(2,1)}, u32[]{:S(2)}, u32[]{:S(2)}) collective-permute-start(bf16[16,576,128]{2,1,0:T(8,128)(2,1)S(1)} %slice_convert_fusion.near), channel_id=1, source_target_pairs={{0,1},{1,0},{2,3},{3,2},{4,5},{5,4},{6,7},{7,6},{8,9},{9,8},{10,11... | collective-permute-start | bytes 7077896 | tf_op jit(solution)/shard_map/ppermute | solution.py:246
  75.9 25.6 %all-to-all-start = ((bf16[16,256,128]{2,1,0:T(8,128)(2,1)}), bf16[16,256,128]{2,1,0:T(8,128)(2,1)S(1)}, u32[]{:S(2)}, u32[]{:S(2)}) async-start(bf16[16,256,128]{2,1,0:T(8,128)(2,1)} %get-tuple-element.14), calls=%async_computation | async-start | bytes 2097152 | tf_op jit(solution)/shard_map/all_to_all | solution.py:237
  102.6 4.3 %copy-start.7 = (f16[2228224]{0:T(1024)(128)(2,1)S(1)}, f16[2228224]{0:T(1024)(128)(2,1)}, u32[]{:S(2)}) copy-start(f16[2228224]{0:T(1024)(128)(2,1)} %copy-done.6) | copy-start | bytes 13369348
  107.0 23.2 %copy-start.2 = (f32[2048]{0:T(1024)S(1)}, f32[2048]{0:T(1024)}, u32[]{:S(2)}) copy-start(f32[2048]{0:T(1024)} %param.23) | copy-start | bytes 24580
  107.0 23.2 %copy-start.3 = (f32[2048]{0:T(1024)S(1)}, f32[2048]{0:T(1024)}, u32[]{:S(2)}) copy-start(f32[2048]{0:T(1024)} %param.24) | copy-start | bytes 24580
  107.4 44.8 %collective-permute-start.1 = (bf16[16,576,128]{2,1,0:T(8,128)(2,1)S(1)}, bf16[16,576,128]{2,1,0:T(8,128)(2,1)}, u32[]{:S(2)}, u32[]{:S(2)}) collective-permute-start(bf16[16,576,128]{2,1,0:T(8,128)(2,1)S(1)} %slice_convert_fusion.1.near), channel_id=1, source_target_pairs={{0,1},{1,0},{2,3},{3,2},{4,5},{5,4},{6,7},{7,6},{8,9},{9,8},{10,11... | collective-permute-start | bytes 7077896 | tf_op jit(solution)/shard_map/ppermute | solution.py:246
  109.4 25.8 %copy-start.10 = (f32[352]{0:T(512)S(1)}, f32[352]{0:T(512)}, u32[]{:S(2)}) copy-start(f32[352]{0:T(512)} %param.26) | copy-start | bytes 4228
  109.4 25.8 %copy-start.11 = (f32[352]{0:T(512)S(1)}, f32[352]{0:T(512)}, u32[]{:S(2)}) copy-start(f32[352]{0:T(512)} %param.28) | copy-start | bytes 4228
  130.5 1.0 copy-start
  131.5 20.7 %all-to-all-start.2 = ((bf16[16,16,2048]{2,1,0:T(8,128)(2,1)}), bf16[16,16,2048]{2,1,0:T(8,128)(2,1)S(1)}, u32[]{:S(2)}, u32[]{:S(2)}) async-start(bf16[16,16,2048]{2,1,0:T(8,128)(2,1)} %copy-done), calls=%async_computation.2 | async-start | bytes 2097152 | tf_op jit(solution)/shard_map/all_to_all | solution.py:237
  152.2 23.4 %copy-start.4 = (f32[2048]{0:T(1024)S(1)}, f32[2048]{0:T(1024)}, u32[]{:S(2)}) copy-start(f32[2048]{0:T(1024)} %param.30) | copy-start | bytes 24580
  152.2 23.4 %copy-start.5 = (f32[2048]{0:T(1024)S(1)}, f32[2048]{0:T(1024)}, u32[]{:S(2)}) copy-start(f32[2048]{0:T(1024)} %param.31) | copy-start | bytes 24580
where the time goes:
time: 188 us; the launch traced here: 187 us
  blocking collectives  119 us (63%)
  waiting for transfers between devices  35.5 us (19%)
  starting transfers between devices  14.5 us (8%)
  Pallas kernels  13 us (7%)
  local copies, waits for them, and re-layouts  3.26 us (2%)
    all_gather x1, blocking collectives, shards(): gathered = lax.all_gather(packed, 'cb_0', axis=0, tiled=True)  68.2 us
    all_to_all x3, blocking collectives, exchange(): return lax.all_to_all(pieces, RA, split_axis=0, concat_axis=0, tiled=True)  50.6 us
    all_to_all x2, waiting for transfers between devices, exchange(): return lax.all_to_all(pieces, RA, split_axis=0, concat_axis=0, tiled=True)  35.5 us
    all_to_all x2, starting transfers between devices, exchange(): return lax.all_to_all(pieces, RA, split_axis=0, concat_axis=0, tiled=True)  10.7 us
    pallas_call x2, Pallas kernels, block(): pl.pallas_call(functools.partial(block_body, start), in_specs=[VMEM, HBM,...  8.48 us
    ppermute x2, starting transfers between devices, both_cores(): return (near, lax.ppermute(near, 'cb_1', ((0, 1), (1, 0))))  3.83 us
  transfers between devices with their start and end apart: 4, of which 2 were waited for; matrix products, arithmetic and copies ran while one was open for 0% of the time, Pallas kernels for 1%

commit v1 on v0

--- a/solution.py
+++ b/solution.py
@@ -136,28 +136,33 @@
     )(pieces, gain[None])
 
 
+def side_by_side(weights, first, last):
+    groups, total, _ = weights.shape
+    rows = total // PART
+    tiles = [
+        weights[:, j * rows : (j + 1) * rows, :].reshape(groups * rows, TILE)
+        for j in range(first, last)
+    ]
+    return jnp.concatenate(tiles, axis=1)
+
+
 def block_body(start, x, near, far, s_gate, s_up, out, held, scales, sems):
-    rows = near.shape[1] // PART
+    pieces = sems.shape[0]
+    groups = held.shape[0] // pieces
     loads = [
-        [
-            pltpu.make_async_copy(
-                weights.at[:, pl.ds(j * rows, rows)],
-                held.at[side, :, :, pl.ds(j * TILE, TILE)],
-                sems.at[side, j],
-            )
-            for side, weights in enumerate((near, far))
-        ]
-        for j in range(PART)
+        pltpu.make_async_copy(
+            far.at[pl.ds(j * groups, groups)], held.at[pl.ds(j * groups, groups)], sems.at[j]
+        )
+        for j in range(pieces)
     ]
-    for pair in loads:
-        for load in pair:
-            load.start()
+    for load in loads:
+        load.start()
     width = s_gate.shape[1]
     scales[...] = jnp.zeros_like(scales)
     scales[0:1, :width] = s_gate[...] / LIFT
     scales[1:2, :width] = s_up[...] / LIFT
-    down = (start + 2 * width) // TILE * TILE
-    place = start + 2 * width - down
+    down = (start + 2 * width) // TILE
+    place = start + 2 * width - down * TILE
     placed = pltpu.roll(scales[...], place, axis=1)
     core = lax.axis_index("cb_1")
     columns = [
@@ -165,12 +170,15 @@
         pl.ds(pl.multiple_of((1 - core) * HALF, HALF), HALF),
     ]
     across = -(-(start + 2 * width) // TILE)
-    both = jnp.zeros((x.shape[0], across * TILE), jnp.float32)
-    for side in (0, 1):
-        for j in range(across):
-            loads[j][side].wait()
-        part = held[side, :, :, : across * TILE].reshape(HALF, across * TILE)
-        both += jnp.dot(x[:, columns[side]], part, preferred_element_type=jnp.float32)
+
+    def product(side, weights):
+        part = side_by_side(weights, 0, across)
+        return jnp.dot(x[:, columns[side]], part, preferred_element_type=jnp.float32)
+
+    both = product(0, near)
+    for load in loads:
+        load.wait()
+    both += product(1, held)
 
     def turned(at):
         return pltpu.roll(both, (place - at) % both.shape[1], axis=1)[:, :WIDE]
@@ -178,27 +186,24 @@
     gate = turned(start) * placed[0:1]
     upper = turned(start + width) * placed[1:2]
     hidden = (gate / (1.0 + jnp.exp(-gate)) * upper).astype(jnp.bfloat16)
-    for side in (0, 1):
-        for j in range(across, PART):
-            loads[j][side].wait()
+    for side, weights in enumerate((near, held)):
         out[:, columns[side]] = lax.dot_general(
             hidden,
-            held[side, :, :, down : down + WIDE].reshape(HALF, WIDE),
+            side_by_side(weights, down, down + WIDE // TILE),
             (((1,), (1,)), ((), ())),
             preferred_element_type=jnp.float32,
         ).astype(jnp.bfloat16)
 
 
 def block(x, near, far, start, s_gate, s_up):
-    groups, rows = near.shape[0], near.shape[1] // PART
     return pl.pallas_call(
         functools.partial(block_body, start),
-        in_specs=[VMEM, HBM, HBM, VMEM, VMEM],
+        in_specs=[VMEM, VMEM, HBM, VMEM, VMEM],
         out_shape=jax.ShapeDtypeStruct(x.shape, jnp.bfloat16),
         scratch_shapes=[
-            pltpu.VMEM((2, groups, rows, PART * TILE), jnp.bfloat16),
+            pltpu.VMEM(far.shape, jnp.bfloat16),
             pltpu.VMEM((8, WIDE), jnp.float32),
-            pltpu.SemaphoreType.DMA((2, PART)),
+            pltpu.SemaphoreType.DMA((4,)),
         ],
         compiler_params=MOST,
     )(x, near, far, s_gate[None], s_up[None])

time: 188 us -> 187 us (level)
  no operation moved by 1% of the time
where the time goes in v1:
time: 187 us
  blocking collectives  119 us (64%)
  waiting for transfers between devices  35.5 us (19%)
  starting transfers between devices  14.5 us (8%)
  Pallas kernels  12.5 us (7%)
  local copies, waits for them, and re-layouts  3.26 us (2%)
  other arithmetic  1.88 us (1%)
    all_gather x1, blocking collectives, shards(): gathered = lax.all_gather(packed, 'cb_0', axis=0, tiled=True)  68.2 us
    all_to_all x3, blocking collectives, exchange(): return lax.all_to_all(pieces, RA, split_axis=0, concat_axis=0, tiled=True)  50.6 us
    all_to_all x2, waiting for transfers between devices, exchange(): return lax.all_to_all(pieces, RA, split_axis=0, concat_axis=0, tiled=True)  35.5 us
    all_to_all x2, starting transfers between devices, exchange(): return lax.all_to_all(pieces, RA, split_axis=0, concat_axis=0, tiled=True)  10.7 us
    pallas_call x2, Pallas kernels, block(): pl.pallas_call(functools.partial(block_body, start), in_specs=[VMEM, VMEM...  7.94 us
    ppermute x2, starting transfers between devices, both_cores(): return (near, lax.ppermute(near, 'cb_1', ((0, 1), (1, 0))))  3.83 us
  transfers between devices with their start and end apart: 4, of which 2 were waited for; matrix products, arithmetic and copies ran while one was open for 0% of the time, Pallas kernels for 1%

profile of v1, /device:TPU:32, one launch (start us, length us, event | category | flops | bytes accessed | tf_op | source)
XLA Modules:
  0.0 186.7 jit_solution(15708751475697405325)
XLA Ops:
  0.0 2.7 %shard_map.154 = (bf16[1088,128]{1,0:T(8,128)(2,1)}, bf16[16,256,128]{2,1,0:T(8,128)(2,1)}) custom-call(f32[64,352]{1,0:T(8,128)} %refs_0_.1, f32[64,352]{1,0:T(8,128)} %refs_1_.1, f32[64,352]{1,0:T(8,128)} %bitcast.25, f32[64,352]{1,0:T(8,128)} %refs_3_.1, f32[64,352]{1,0:T(8,128)} %refs_4_.1, f32[64,352]{1,0:T(8,128)} %bitcast.26, bf16[256,128]{1,0:T(8,128)(2,1)} %refs_6_.1), custom_call_target="tpu_custom_call" | custom-call | tf_op jit(solution)/shard_map/pallas_call | solution.py:62
  2.7 1.0 convert_bitcast_fusion
  3.7 68.2 %all-gather.1 = f16[2228224]{0:T(1024)(128)(2,1)S(1)} all-gather(f16[139264]{0:T(1024)(128)(2,1)S(1)} %convert_bitcast_fusion), channel_id=1, replica_groups=mesh['ra_0'=4,'ra_1'=4,'cb_0'=16,'cb_1'=2] {'cb_0'}, dimensions={0}, use_global_device_ids=true | all-gather | bytes 4734976 | tf_op jit(solution)/shard_map/all_gather | solution.py:277
  71.9 0.0 copy-start.6
  71.9 0.0 copy-start.8
  71.9 0.0 copy-start.9
  71.9 0.0 copy-start.1
  71.9 0.4 slice_convert_fusion.near
  72.4 1.6 copy-done.6
  73.9 1.9 %collective-permute-start = (bf16[16,576,128]{2,1,0:T(8,128)(2,1)S(1)}, bf16[16,576,128]{2,1,0:T(8,128)(2,1)}, u32[]{:S(2)}, u32[]{:S(2)}) collective-permute-start(bf16[16,576,128]{2,1,0:T(8,128)(2,1)S(1)} %slice_convert_fusion.near), channel_id=1, source_target_pairs={{0,1},{1,0},{2,3},{3,2},{4,5},{5,4},{6,7},{7,6},{8,9},{9,8},{10,11... | collective-permute-start | bytes 7077896 | tf_op jit(solution)/shard_map/ppermute | solution.py:251
  75.9 7.0 %all-to-all-start = ((bf16[16,256,128]{2,1,0:T(8,128)(2,1)}), bf16[16,256,128]{2,1,0:T(8,128)(2,1)S(1)}, u32[]{:S(2)}, u32[]{:S(2)}) async-start(bf16[16,256,128]{2,1,0:T(8,128)(2,1)} %get-tuple-element.14), calls=%async_computation | async-start | bytes 2097152 | tf_op jit(solution)/shard_map/all_to_all | solution.py:242
  82.9 0.0 copy-done.8
  82.9 0.0 copy-done.9
  83.0 18.5 %all-to-all-done.pieces = bf16[16,256,128]{2,1,0:T(8,128)(2,1)S(1)} async-done(((bf16[16,256,128]{2,1,0:T(8,128)(2,1)}), bf16[16,256,128]{2,1,0:T(8,128)(2,1)S(1)}, u32[]{:S(2)}, u32[]{:S(2)}) %all-to-all-start) | async-done | bytes 1048608 | tf_op jit(solution)/shard_map/all_to_all | solution.py:242
  101.5 0.0 copy-done.1
  101.5 1.1 shard_map.155
  102.6 0.0 collective-permute-done.far
  102.6 0.0 copy-start.7
  102.7 4.0 %shard_map.156 = bf16[256,2048]{1,0:T(8,128)(2,1)S(1)} custom-call(bf16[256,2048]{1,0:T(8,128)(2,1)S(1)} %get-tuple-element.15.x, bf16[16,576,128]{2,1,0:T(8,128)(2,1)S(1)} %slice_convert_fusion.near, bf16[16,576,128]{2,1,0:T(8,128)(2,1)} %collective-permute-done.far, f32[1,352]{1,0:T(1,128)S(1)} %broadcast_in_dim.28.s_gate, f32[1,352]{1,0:T(1,128)S(1)} %broadcast_in_dim.29.s_up), custom_call_target="tpu_custom_call" | custom-call | tf_op jit(solution)/shard_map/pallas_call | solution.py:199
  106.7 0.0 copy-done.7
  106.7 0.0 copy-start.2
  106.7 0.0 copy-start.3
  106.7 0.4 slice_convert_fusion.1.near
  107.2 1.9 %collective-permute-start.1 = (bf16[16,576,128]{2,1,0:T(8,128)(2,1)S(1)}, bf16[16,576,128]{2,1,0:T(8,128)(2,1)}, u32[]{:S(2)}, u32[]{:S(2)}) collective-permute-start(bf16[16,576,128]{2,1,0:T(8,128)(2,1)S(1)} %slice_convert_fusion.1.near), channel_id=1, source_target_pairs={{0,1},{1,0},{2,3},{3,2},{4,5},{5,4},{6,7},{7,6},{8,9},{9,8},{10,11... | collective-permute-start | bytes 7077896 | tf_op jit(solution)/shard_map/ppermute | solution.py:251
  109.1 0.0 copy-start.10
  109.1 0.0 copy-start.11
  109.1 20.8 %all_to_all.25.pieces = bf16[16,16,2048]{2,1,0:T(8,128)(2,1)S(1)} all-to-all(bf16[16,16,2048]{2,1,0:T(8,128)(2,1)S(1)} %bitcast.15), channel_id=1, replica_groups=mesh['ra_0'=4,'ra_1'=4,'cb_0'=16,'cb_1'=2] {'ra_0','ra_1'}, dimensions={0} | all-to-all | bytes 2097152 | tf_op jit(solution)/shard_map/all_to_all | solution.py:242
  129.9 0.0 copy-done.2
  129.9 0.0 copy-done.3
  129.9 0.3 shard_map.157
  130.2 0.0 copy-start
  130.2 1.0 copy-done
  131.2 3.7 %all-to-all-start.2 = ((bf16[16,16,2048]{2,1,0:T(8,128)(2,1)}), bf16[16,16,2048]{2,1,0:T(8,128)(2,1)S(1)}, u32[]{:S(2)}, u32[]{:S(2)}) async-start(bf16[16,16,2048]{2,1,0:T(8,128)(2,1)} %copy-done), calls=%async_computation.2 | async-start | bytes 2097152 | tf_op jit(solution)/shard_map/all_to_all | solution.py:242
  134.9 0.0 copy-done.10
  134.9 0.0 copy-done.11
  134.9 17.0 %all-to-all-done.2 = bf16[16,16,2048]{2,1,0:T(8,128)(2,1)S(1)} async-done(((bf16[16,16,2048]{2,1,0:T(8,128)(2,1)}), bf16[16,16,2048]{2,1,0:T(8,128)(2,1)S(1)}, u32[]{:S(2)}, u32[]{:S(2)}) %all-to-all-start.2) | async-done | bytes 1048608 | tf_op jit(solution)/shard_map/all_to_all | solution.py:242
  151.9 0.0 collective-permute-done.1.far
  151.9 0.0 copy-start.4
  151.9 0.0 copy-start.5
  151.9 3.9 %shard_map.158 = bf16[256,2048]{1,0:T(8,128)(2,1)S(1)} custom-call(bf16[256,2048]{1,0:T(8,128)(2,1)S(1)} %bitcast.14, bf16[16,576,128]{2,1,0:T(8,128)(2,1)S(1)} %slice_convert_fusion.1.near, bf16[16,576,128]{2,1,0:T(8,128)(2,1)} %collective-permute-done.1.far, f32[1,352]{1,0:T(1,128)S(1)} %broadcast_in_dim.32.s_gate, f32[1,352]{1,0:T(1,128)S(1)} %broadcast_in_dim.33.s_up), custom_call_target="tpu_custom_call" | custom-call | tf_op jit(solution)/shard_map/pallas_call | solution.py:199
  155.8 19.2 %all_to_all.26.pieces = bf16[16,16,2048]{2,1,0:T(8,128)(2,1)S(1)} all-to-all(bf16[16,16,2048]{2,1,0:T(8,128)(2,1)S(1)} %bitcast.16), channel_id=1, replica_groups=mesh['ra_0'=4,'ra_1'=4,'cb_0'=16,'cb_1'=2] {'ra_0','ra_1'}, dimensions={0} | all-to-all | bytes 2097152 | tf_op jit(solution)/shard_map/all_to_all | solution.py:242
  175.0 0.0 copy-done.4
  175.0 0.0 copy-done.5
  175.1 0.3 shard_map.159
  175.4 10.6 %all_to_all.27 = bf16[16,16,128]{2,1,0:T(8,128)(2,1)S(1)} all-to-all(bf16[16,16,128]{2,1,0:T(8,128)(2,1)S(1)} %shard_map.159), channel_id=1, replica_groups=mesh['ra_0'=4,'ra_1'=4,'cb_0'=16,'cb_1'=2] {'ra_0','ra_1'}, dimensions={0} | all-to-all | bytes 131072 | tf_op jit(solution)/shard_map/all_to_all | solution.py:242
  186.0 0.6 copy.18
  (4 shorter events, 0.0 us)
Async XLA Ops:
  71.9 2.0 %copy-start.6 = (f16[2228224]{0:T(1024)(128)(2,1)}, f16[2228224]{0:T(1024)(128)(2,1)S(1)}, u32[]{:S(2)}) copy-start(f16[2228224]{0:T(1024)(128)(2,1)S(1)} %all-gather.1) | copy-start | bytes 13369348
  71.9 11.0 %copy-start.8 = (f32[352]{0:T(512)S(1)}, f32[352]{0:T(512)}, u32[]{:S(2)}) copy-start(f32[352]{0:T(512)} %param.19) | copy-start | bytes 4228
  71.9 11.0 %copy-start.9 = (f32[352]{0:T(512)S(1)}, f32[352]{0:T(512)}, u32[]{:S(2)}) copy-start(f32[352]{0:T(512)} %param.21) | copy-start | bytes 4228
  71.9 29.6 %copy-start.1 = (f32[2048]{0:T(1024)S(1)}, f32[2048]{0:T(1024)}, u32[]{:S(2)}) copy-start(f32[2048]{0:T(1024)} %param.17) | copy-start | bytes 24580
  73.9 28.7 %collective-permute-start = (bf16[16,576,128]{2,1,0:T(8,128)(2,1)S(1)}, bf16[16,576,128]{2,1,0:T(8,128)(2,1)}, u32[]{:S(2)}, u32[]{:S(2)}) collective-permute-start(bf16[16,576,128]{2,1,0:T(8,128)(2,1)S(1)} %slice_convert_fusion.near), channel_id=1, source_target_pairs={{0,1},{1,0},{2,3},{3,2},{4,5},{5,4},{6,7},{7,6},{8,9},{9,8},{10,11... | collective-permute-start | bytes 7077896 | tf_op jit(solution)/shard_map/ppermute | solution.py:251
  75.9 25.6 %all-to-all-start = ((bf16[16,256,128]{2,1,0:T(8,128)(2,1)}), bf16[16,256,128]{2,1,0:T(8,128)(2,1)S(1)}, u32[]{:S(2)}, u32[]{:S(2)}) async-start(bf16[16,256,128]{2,1,0:T(8,128)(2,1)} %get-tuple-element.14), calls=%async_computation | async-start | bytes 2097152 | tf_op jit(solution)/shard_map/all_to_all | solution.py:242
  102.6 4.1 %copy-start.7 = (f16[2228224]{0:T(1024)(128)(2,1)S(1)}, f16[2228224]{0:T(1024)(128)(2,1)}, u32[]{:S(2)}) copy-start(f16[2228224]{0:T(1024)(128)(2,1)} %copy-done.6) | copy-start | bytes 13369348
  106.7 23.2 %copy-start.2 = (f32[2048]{0:T(1024)S(1)}, f32[2048]{0:T(1024)}, u32[]{:S(2)}) copy-start(f32[2048]{0:T(1024)} %param.23) | copy-start | bytes 24580
  106.7 23.2 %copy-start.3 = (f32[2048]{0:T(1024)S(1)}, f32[2048]{0:T(1024)}, u32[]{:S(2)}) copy-start(f32[2048]{0:T(1024)} %param.24) | copy-start | bytes 24580
  107.2 44.8 %collective-permute-start.1 = (bf16[16,576,128]{2,1,0:T(8,128)(2,1)S(1)}, bf16[16,576,128]{2,1,0:T(8,128)(2,1)}, u32[]{:S(2)}, u32[]{:S(2)}) collective-permute-start(bf16[16,576,128]{2,1,0:T(8,128)(2,1)S(1)} %slice_convert_fusion.1.near), channel_id=1, source_target_pairs={{0,1},{1,0},{2,3},{3,2},{4,5},{5,4},{6,7},{7,6},{8,9},{9,8},{10,11... | collective-permute-start | bytes 7077896 | tf_op jit(solution)/shard_map/ppermute | solution.py:251
  109.1 25.8 %copy-start.10 = (f32[352]{0:T(512)S(1)}, f32[352]{0:T(512)}, u32[]{:S(2)}) copy-start(f32[352]{0:T(512)} %param.26) | copy-start | bytes 4228
  109.1 25.8 %copy-start.11 = (f32[352]{0:T(512)S(1)}, f32[352]{0:T(512)}, u32[]{:S(2)}) copy-start(f32[352]{0:T(512)} %param.28) | copy-start | bytes 4228
  130.2 1.0 copy-start
  131.2 20.7 %all-to-all-start.2 = ((bf16[16,16,2048]{2,1,0:T(8,128)(2,1)}), bf16[16,16,2048]{2,1,0:T(8,128)(2,1)S(1)}, u32[]{:S(2)}, u32[]{:S(2)}) async-start(bf16[16,16,2048]{2,1,0:T(8,128)(2,1)} %copy-done), calls=%async_computation.2 | async-start | bytes 2097152 | tf_op jit(solution)/shard_map/all_to_all | solution.py:242
  151.9 23.1 %copy-start.4 = (f32[2048]{0:T(1024)S(1)}, f32[2048]{0:T(1024)}, u32[]{:S(2)}) copy-start(f32[2048]{0:T(1024)} %param.30) | copy-start | bytes 24580
  151.9 23.1 %copy-start.5 = (f32[2048]{0:T(1024)S(1)}, f32[2048]{0:T(1024)}, u32[]{:S(2)}) copy-start(f32[2048]{0:T(1024)} %param.31) | copy-start | bytes 24580

commit v2 on v1

--- a/solution.py
+++ b/solution.py
@@ -20,7 +20,6 @@
 EPS = 1e-06
 LIFT = 2.0**18
 ROOM = pltpu.CompilerParams(vmem_limit_bytes=20 * 1024 * 1024)
-MOST = pltpu.CompilerParams(vmem_limit_bytes=24 * 1024 * 1024)
 VMEM = pl.BlockSpec(memory_space=pltpu.VMEM)
 HBM = pl.BlockSpec(memory_space=pltpu.HBM)
 
@@ -136,27 +135,24 @@
     )(pieces, gain[None])
 
 
-def side_by_side(weights, first, last):
-    groups, total, _ = weights.shape
+def side_by_side(weights, side, first, last):
+    groups, _, total, _ = weights.shape
     rows = total // PART
     tiles = [
-        weights[:, j * rows : (j + 1) * rows, :].reshape(groups * rows, TILE)
+        weights[:, side, j * rows : (j + 1) * rows, :].reshape(groups * rows, TILE)
         for j in range(first, last)
     ]
     return jnp.concatenate(tiles, axis=1)
 
 
-def block_body(start, x, near, far, s_gate, s_up, out, held, scales, sems):
-    pieces = sems.shape[0]
-    groups = held.shape[0] // pieces
-    loads = [
-        pltpu.make_async_copy(
-            far.at[pl.ds(j * groups, groups)], held.at[pl.ds(j * groups, groups)], sems.at[j]
-        )
-        for j in range(pieces)
+def block_body(start, x, s_gate, s_up, *refs):
+    parts, (out, scales) = refs[:-2], refs[-2:]
+    share = HALF // len(parts)
+    places = [
+        (part, side, slice(side * HALF + p * share, side * HALF + (p + 1) * share))
+        for p, part in enumerate(parts)
+        for side in (0, 1)
     ]
-    for load in loads:
-        load.start()
     width = s_gate.shape[1]
     scales[...] = jnp.zeros_like(scales)
     scales[0:1, :width] = s_gate[...] / LIFT
@@ -164,21 +160,12 @@
     down = (start + 2 * width) // TILE
     place = start + 2 * width - down * TILE
     placed = pltpu.roll(scales[...], place, axis=1)
-    core = lax.axis_index("cb_1")
-    columns = [
-        pl.ds(pl.multiple_of(core * HALF, HALF), HALF),
-        pl.ds(pl.multiple_of((1 - core) * HALF, HALF), HALF),
-    ]
     across = -(-(start + 2 * width) // TILE)
 
-    def product(side, weights):
-        part = side_by_side(weights, 0, across)
-        return jnp.dot(x[:, columns[side]], part, preferred_element_type=jnp.float32)
-
-    both = product(0, near)
-    for load in loads:
-        load.wait()
-    both += product(1, held)
+    both = jnp.zeros((x.shape[0], across * TILE), jnp.float32)
+    for part, side, at in places:
+        tiles = side_by_side(part, side, 0, across)
+        both += jnp.dot(x[:, at], tiles, preferred_element_type=jnp.float32)
 
     def turned(at):
         return pltpu.roll(both, (place - at) % both.shape[1], axis=1)[:, :WIDE]
@@ -186,27 +173,22 @@
     gate = turned(start) * placed[0:1]
     upper = turned(start + width) * placed[1:2]
     hidden = (gate / (1.0 + jnp.exp(-gate)) * upper).astype(jnp.bfloat16)
-    for side, weights in enumerate((near, held)):
-        out[:, columns[side]] = lax.dot_general(
+    for part, side, at in places:
+        out[:, at] = lax.dot_general(
             hidden,
-            side_by_side(weights, down, down + WIDE // TILE),
+            side_by_side(part, side, down, down + WIDE // TILE),
             (((1,), (1,)), ((), ())),
             preferred_element_type=jnp.float32,
         ).astype(jnp.bfloat16)
 
 
-def block(x, near, far, start, s_gate, s_up):
+def block(x, parts, start, s_gate, s_up):
     return pl.pallas_call(
         functools.partial(block_body, start),
-        in_specs=[VMEM, VMEM, HBM, VMEM, VMEM],
         out_shape=jax.ShapeDtypeStruct(x.shape, jnp.bfloat16),
-        scratch_shapes=[
-            pltpu.VMEM(far.shape, jnp.bfloat16),
-            pltpu.VMEM((8, WIDE), jnp.float32),
-            pltpu.SemaphoreType.DMA((4,)),
-        ],
-        compiler_params=MOST,
-    )(x, near, far, s_gate[None], s_up[None])
+        scratch_shapes=[pltpu.VMEM((8, WIDE), jnp.float32)],
+        compiler_params=ROOM,
+    )(x, s_gate[None], s_up[None], *parts)
 
 
 def join_body(last, pieces, before, scale, gain, *outs):
@@ -246,9 +228,8 @@
     return exchange(partial_value.reshape(lax.axis_size(RA), -1, D))
 
 
-def both_cores(weights):
-    near = weights.astype(jnp.bfloat16)
-    return near, lax.ppermute(near, "cb_1", ((0, 1), (1, 0)))
+def in_parts(weights):
+    return [part.astype(jnp.bfloat16) for part in jnp.split(weights, 2, axis=0)]
 
 
 def shards(
@@ -274,19 +255,19 @@
     )
     pieces = exchange(copies)
     packed = packed.reshape(-1).astype(jnp.float16)
-    gathered = lax.all_gather(packed, "cb_0", axis=0, tiled=True)
+    gathered = lax.all_gather(packed, CB, axis=0, tiled=True)
     rows, width = gate_first.shape
-    weights = gathered.reshape(-1, TILES * rows, TILE)
+    weights = gathered.reshape(-1, 2, TILES * rows, TILE)
     later, start = divmod(3 * width, TILE)
-    near, far = both_cores(weights[:, : PART * rows])
+    earlier = in_parts(weights[:, :, : PART * rows])
     normed, own = spread(pieces, gain_first)
-    partial_first = block(normed, near, far, 0, gate_first_scale, up_first_scale)
+    partial_first = block(normed, earlier, 0, gate_first_scale, up_first_scale)
     weights, partial_first = lax.optimization_barrier((weights, partial_first))
-    near, far = both_cores(weights[:, later * rows :])
+    second = in_parts(weights[:, :, later * rows :])
     arrived = by_rows(partial_first)
     copies, first = join(arrived, own, down_first_scale, gain_second, False)
     normed = exchange(copies).reshape(-1, D)
-    partial_second = block(normed, near, far, start, gate_second_scale, up_second_scale)
+    partial_second = block(normed, second, start, gate_second_scale, up_second_scale)
     (columns,) = join(by_rows(partial_second), first, down_second_scale, gain_last, True)
     return exchange(columns).reshape(tokens.shape)
 

time: 187 us -> 172 us (0.920)
  waiting for transfers between devices: 35.5 us -> 12.2 us
  other arithmetic: 1.88 us -> 7.95 us
  local copies, waits for them, and re-layouts: 3.26 us -> 7.44 us
  blocking collectives: 119 us -> 123 us
  starting transfers between devices: 14.5 us -> 10.7 us
  Pallas kernels: 12.5 us -> 10 us
    all_to_all x2, waiting for transfers between devices: 35.5 us -> 12.2 us  [exchange(): return lax.all_to_all(pieces, RA, split_axis=0, concat_axis=0, tiled=True)]
    convert_element_type x2, other arithmetic: 0.87 us -> 6.95 us  [in_parts(): return [part.astype(jnp.bfloat16) for part in jnp.split(weights, 2, axis=0)]]
    all_to_all x3, blocking collectives: 50.6 us -> 54.9 us  [exchange(): return lax.all_to_all(pieces, RA, split_axis=0, concat_axis=0, tiled=True)]
    unnamed x25, local copies, waits for them, and re-layouts: 3.25 us -> 7.43 us
    ppermute x2 -> x0, starting transfers between devices: 3.83 us -> none  [both_cores(): return (near, lax.ppermute(near, 'cb_1', ((0, 1), (1, 0))))]
    pallas_call x2, Pallas kernels: 7.94 us -> 4.52 us  [block(): pl.pallas_call(functools.partial(block_body, start), out_shape=jax.ShapeD...]
  transfers between devices with their start and end apart: 4 -> 2, of which waited for: 2 -> 1; matrix products, arithmetic and copies ran while one was open for 0% -> 5% of each run, Pallas kernels for 1% -> 0%
where the time goes in v2:
time: 172 us
  blocking collectives  123 us (72%)
  waiting for transfers between devices  12.2 us (7%)
  starting transfers between devices  10.7 us (6%)
  Pallas kernels  10 us (6%)
  other arithmetic  7.95 us (5%)
  local copies, waits for them, and re-layouts  7.44 us (4%)
    all_gather x1, blocking collectives, shards(): gathered = lax.all_gather(packed, CB, axis=0, tiled=True)  68.2 us
    all_to_all x3, blocking collectives, exchange(): return lax.all_to_all(pieces, RA, split_axis=0, concat_axis=0, tiled=True)  54.9 us
    all_to_all x2, waiting for transfers between devices, exchange(): return lax.all_to_all(pieces, RA, split_axis=0, concat_axis=0, tiled=True)  12.2 us
    all_to_all x2, starting transfers between devices, exchange(): return lax.all_to_all(pieces, RA, split_axis=0, concat_axis=0, tiled=True)  10.7 us
    unnamed x25, local copies, waits for them, and re-layouts  7.43 us
    convert_element_type x2, other arithmetic, in_parts(): return [part.astype(jnp.bfloat16) for part in jnp.split(weights, 2, axis=0)]  6.95 us
    pallas_call x2, Pallas kernels, block(): pl.pallas_call(functools.partial(block_body, start), out_shape=jax.ShapeD...  4.52 us
  transfers between devices with their start and end apart: 2, of which 1 were waited for; matrix products, arithmetic and copies ran while one was open for 5% of the time, Pallas kernels for 0%

profile of v2, /device:TPU:32, one launch (start us, length us, event | category | flops | bytes accessed | tf_op | source)
XLA Modules:
  0.0 171.6 jit_solution(16745622645798865574)
XLA Ops:
  0.0 2.7 %shard_map.154 = (bf16[1088,128]{1,0:T(8,128)(2,1)}, bf16[16,256,128]{2,1,0:T(8,128)(2,1)}) custom-call(f32[64,352]{1,0:T(8,128)} %refs_0_.1, f32[64,352]{1,0:T(8,128)} %refs_1_.1, f32[64,352]{1,0:T(8,128)} %bitcast.25, f32[64,352]{1,0:T(8,128)} %refs_3_.1, f32[64,352]{1,0:T(8,128)} %refs_4_.1, f32[64,352]{1,0:T(8,128)} %bitcast.26, bf16[256,128]{1,0:T(8,128)(2,1)} %refs_6_.1), custom_call_target="tpu_custom_call" | custom-call | tf_op jit(solution)/shard_map/pallas_call | solution.py:61
  2.7 7.0 %all-to-all-start = ((bf16[16,256,128]{2,1,0:T(8,128)(2,1)}), bf16[16,256,128]{2,1,0:T(8,128)(2,1)S(1)}, u32[]{:S(2)}, u32[]{:S(2)}) async-start(bf16[16,256,128]{2,1,0:T(8,128)(2,1)} %get-tuple-element.14), calls=%async_computation | async-start | bytes 2097152 | tf_op jit(solution)/shard_map/all_to_all | solution.py:224
  9.8 1.0 convert_bitcast_fusion
  10.8 0.0 copy-start.8
  10.8 0.0 copy-start.9
  10.8 68.2 %all-gather.1 = f16[4456448]{0:T(1024)(128)(2,1)S(1)} all-gather(f16[139264]{0:T(1024)(128)(2,1)S(1)} %convert_bitcast_fusion), channel_id=1, replica_groups=mesh['ra_0'=4,'ra_1'=4,'cb_0'=16,'cb_1'=2] {'cb_0','cb_1'}, dimensions={0}, use_global_device_ids=true | all-gather | bytes 9191424 | tf_op jit(solution)/shard_map/all_gather | solution.py:258
  79.0 0.0 copy-done.8
  79.0 0.0 copy-start.7
  79.0 0.0 copy-done.9
  79.0 3.4 %copy-done.7 = f16[4456448]{0:T(1024)(128)(2,1)} copy-done((f16[4456448]{0:T(1024)(128)(2,1)}, f16[4456448]{0:T(1024)(128)(2,1)S(1)}, u32[]{:S(2)}) %copy-start.7) | copy-done | bytes 8912920
  82.5 0.0 copy-start.2
  82.5 2.4 %slice_convert_fusion = (bf16[8,2,576,128]{3,2,1,0:T(8,128)(2,1)S(1)}, bf16[8,2,576,128]{3,2,1,0:T(8,128)(2,1)}) fusion(f16[16,2,1088,128]{3,2,1,0:T(8,128)(2,1)S(1)} %bitcast.22), kind=kLoop, calls=%fused_computation | loop fusion | flops 2359296 | bytes 9437184 | tf_op jit(solution)/shard_map/convert_element_type | solution.py:232
  84.8 0.0 all-to-all-done.pieces
  84.8 0.0 copy-done.2
  84.8 1.1 shard_map.155
  86.0 0.0 copy-start
  86.0 1.7 copy-done
  87.6 0.0 copy-start.3
  87.6 0.0 copy-start.4
  87.6 2.3 %shard_map.156 = bf16[256,2048]{1,0:T(8,128)(2,1)S(1)} custom-call(bf16[256,2048]{1,0:T(8,128)(2,1)S(1)} %get-tuple-element.15.x, f32[1,352]{1,0:T(1,128)S(1)} %broadcast_in_dim.28.s_gate, f32[1,352]{1,0:T(1,128)S(1)} %broadcast_in_dim.29.s_up, bf16[8,2,576,128]{3,2,1,0:T(8,128)(2,1)S(1)} %copy-done, bf16[8,2,576,128]{3,2,1,0:T(8,128)(2,1)S(1)} %get-tuple-element.23.refs_1_), custom_call_target="tpu_custom_call" | custom-call | tf_op jit(solution)/shard_map/pallas_call | solution.py:186
  89.9 0.0 copy-start.10
  89.9 0.0 copy-start.11
  89.9 25.0 %all_to_all.25.pieces = bf16[16,16,2048]{2,1,0:T(8,128)(2,1)S(1)} all-to-all(bf16[16,16,2048]{2,1,0:T(8,128)(2,1)S(1)} %bitcast.15), channel_id=1, replica_groups=mesh['ra_0'=4,'ra_1'=4,'cb_0'=16,'cb_1'=2] {'ra_0','ra_1'}, dimensions={0} | all-to-all | bytes 2097152 | tf_op jit(solution)/shard_map/all_to_all | solution.py:224
  114.9 0.0 copy-done.3
  114.9 0.0 copy-done.4
  114.9 1.3 shard_map.157
  116.2 3.7 %all-to-all-start.2 = ((bf16[16,16,2048]{2,1,0:T(8,128)(2,1)}), bf16[16,16,2048]{2,1,0:T(8,128)(2,1)S(1)}, u32[]{:S(2)}, u32[]{:S(2)}) async-start(bf16[16,16,2048]{2,1,0:T(8,128)(2,1)} %get-tuple-element.18), calls=%async_computation.2 | async-start | bytes 2097152 | tf_op jit(solution)/shard_map/all_to_all | solution.py:224
  119.9 0.0 copy-done.10
  119.9 0.0 copy-done.11
  119.9 4.6 %slice_convert_fusion.2 = (bf16[8,2,576,128]{3,2,1,0:T(8,128)(2,1)S(1)}, bf16[8,2,576,128]{3,2,1,0:T(8,128)(2,1)}) fusion(f16[16,2,1088,128]{3,2,1,0:T(8,128)(2,1)} %bitcast.23), kind=kLoop, calls=%fused_computation.2 | loop fusion | flops 2359296 | bytes 9437184 | tf_op jit(solution)/shard_map/convert_element_type | solution.py:232
  124.5 12.2 %all-to-all-done.2 = bf16[16,16,2048]{2,1,0:T(8,128)(2,1)S(1)} async-done(((bf16[16,16,2048]{2,1,0:T(8,128)(2,1)}), bf16[16,16,2048]{2,1,0:T(8,128)(2,1)S(1)}, u32[]{:S(2)}, u32[]{:S(2)}) %all-to-all-start.2) | async-done | bytes 1048608 | tf_op jit(solution)/shard_map/all_to_all | solution.py:224
  136.7 0.0 copy-start.1
  136.7 1.7 copy-done.1
  138.4 0.0 copy-start.5
  138.4 0.0 copy-start.6
  138.4 2.3 %shard_map.158 = bf16[256,2048]{1,0:T(8,128)(2,1)S(1)} custom-call(bf16[256,2048]{1,0:T(8,128)(2,1)S(1)} %bitcast.14, f32[1,352]{1,0:T(1,128)S(1)} %broadcast_in_dim.32.s_gate, f32[1,352]{1,0:T(1,128)S(1)} %broadcast_in_dim.33.s_up, bf16[8,2,576,128]{3,2,1,0:T(8,128)(2,1)S(1)} %copy-done.1, bf16[8,2,576,128]{3,2,1,0:T(8,128)(2,1)S(1)} %get-tuple-element.21.refs_1_), custom_call_target="tpu_custom_call" | custom-call | tf_op jit(solution)/shard_map/pallas_call | solution.py:186
  140.7 19.4 %all_to_all.26.pieces = bf16[16,16,2048]{2,1,0:T(8,128)(2,1)S(1)} all-to-all(bf16[16,16,2048]{2,1,0:T(8,128)(2,1)S(1)} %bitcast.16), channel_id=1, replica_groups=mesh['ra_0'=4,'ra_1'=4,'cb_0'=16,'cb_1'=2] {'ra_0','ra_1'}, dimensions={0} | all-to-all | bytes 2097152 | tf_op jit(solution)/shard_map/all_to_all | solution.py:224
  160.0 0.0 copy-done.5
  160.0 0.0 copy-done.6
  160.0 0.3 shard_map.159
  160.4 10.6 %all_to_all.27 = bf16[16,16,128]{2,1,0:T(8,128)(2,1)S(1)} all-to-all(bf16[16,16,128]{2,1,0:T(8,128)(2,1)S(1)} %shard_map.159), channel_id=1, replica_groups=mesh['ra_0'=4,'ra_1'=4,'cb_0'=16,'cb_1'=2] {'ra_0','ra_1'}, dimensions={0} | all-to-all | bytes 131072 | tf_op jit(solution)/shard_map/all_to_all | solution.py:224
  171.0 0.6 copy.18
  (4 shorter events, 0.0 us)
Async XLA Ops:
  2.7 82.1 %all-to-all-start = ((bf16[16,256,128]{2,1,0:T(8,128)(2,1)}), bf16[16,256,128]{2,1,0:T(8,128)(2,1)S(1)}, u32[]{:S(2)}, u32[]{:S(2)}) async-start(bf16[16,256,128]{2,1,0:T(8,128)(2,1)} %get-tuple-element.14), calls=%async_computation | async-start | bytes 2097152 | tf_op jit(solution)/shard_map/all_to_all | solution.py:224
  10.8 68.2 %copy-start.8 = (f32[352]{0:T(512)S(1)}, f32[352]{0:T(512)}, u32[]{:S(2)}) copy-start(f32[352]{0:T(512)} %param.19) | copy-start | bytes 4228
  10.8 68.2 %copy-start.9 = (f32[352]{0:T(512)S(1)}, f32[352]{0:T(512)}, u32[]{:S(2)}) copy-start(f32[352]{0:T(512)} %param.21) | copy-start | bytes 4228
  79.0 3.4 %copy-start.7 = (f16[4456448]{0:T(1024)(128)(2,1)}, f16[4456448]{0:T(1024)(128)(2,1)S(1)}, u32[]{:S(2)}) copy-start(f16[4456448]{0:T(1024)(128)(2,1)S(1)} %all-gather.1) | copy-start | bytes 26738692
  82.5 2.4 %copy-start.2 = (f32[2048]{0:T(1024)S(1)}, f32[2048]{0:T(1024)}, u32[]{:S(2)}) copy-start(f32[2048]{0:T(1024)} %param.17) | copy-start | bytes 24580
  86.0 1.7 copy-start
  87.6 27.3 %copy-start.3 = (f32[2048]{0:T(1024)S(1)}, f32[2048]{0:T(1024)}, u32[]{:S(2)}) copy-start(f32[2048]{0:T(1024)} %param.23) | copy-start | bytes 24580
  87.6 27.3 %copy-start.4 = (f32[2048]{0:T(1024)S(1)}, f32[2048]{0:T(1024)}, u32[]{:S(2)}) copy-start(f32[2048]{0:T(1024)} %param.24) | copy-start | bytes 24580
  89.9 30.0 %copy-start.10 = (f32[352]{0:T(512)S(1)}, f32[352]{0:T(512)}, u32[]{:S(2)}) copy-start(f32[352]{0:T(512)} %param.26) | copy-start | bytes 4228
  89.9 30.0 %copy-start.11 = (f32[352]{0:T(512)S(1)}, f32[352]{0:T(512)}, u32[]{:S(2)}) copy-start(f32[352]{0:T(512)} %param.28) | copy-start | bytes 4228
  116.2 20.5 %all-to-all-start.2 = ((bf16[16,16,2048]{2,1,0:T(8,128)(2,1)}), bf16[16,16,2048]{2,1,0:T(8,128)(2,1)S(1)}, u32[]{:S(2)}, u32[]{:S(2)}) async-start(bf16[16,16,2048]{2,1,0:T(8,128)(2,1)} %get-tuple-element.18), calls=%async_computation.2 | async-start | bytes 2097152 | tf_op jit(solution)/shard_map/all_to_all | solution.py:224
  136.7 1.7 copy-start.1
  138.4 21.6 %copy-start.5 = (f32[2048]{0:T(1024)S(1)}, f32[2048]{0:T(1024)}, u32[]{:S(2)}) copy-start(f32[2048]{0:T(1024)} %param.30) | copy-start | bytes 24580
  138.4 21.6 %copy-start.6 = (f32[2048]{0:T(1024)S(1)}, f32[2048]{0:T(1024)}, u32[]{:S(2)}) copy-start(f32[2048]{0:T(1024)} %param.31) | copy-start | bytes 24580

commit v3 on v2

--- a/solution.py
+++ b/solution.py
@@ -17,6 +17,7 @@
 TILES = 17
 PART = 9
 WIDE = 4 * TILE
+PARTS = 4
 EPS = 1e-06
 LIFT = 2.0**18
 ROOM = pltpu.CompilerParams(vmem_limit_bytes=20 * 1024 * 1024)
@@ -229,7 +230,13 @@
 
 
 def in_parts(weights):
-    return [part.astype(jnp.bfloat16) for part in jnp.split(weights, 2, axis=0)]
+    parts, count = [], PARTS
+    size = weights.shape[0] // count
+    for j in range(count):
+        part = weights[j * size : (j + 1) * size].astype(jnp.bfloat16)
+        weights, part = lax.optimization_barrier((weights, part))
+        parts.append(part)
+    return parts
 
 
 def shards(

time: 172 us -> 177 us (1.029)
  blocking collectives: 123 us -> 98.9 us
  waiting for transfers between devices: 12.2 us -> 27.9 us
  starting transfers between devices: 10.7 us -> 18.8 us
  local copies, waits for them, and re-layouts: 7.44 us -> 12.3 us
  other arithmetic: 7.95 us -> 5.07 us
  Pallas kernels: 10 us -> 12.5 us
    all_to_all x3 -> x2, blocking collectives: 54.9 us -> 30.5 us  [exchange(): return lax.all_to_all(pieces, RA, split_axis=0, concat_axis=0, tiled=True)]
    all_to_all x2 -> x3, waiting for transfers between devices: 12.2 us -> 27.9 us  [exchange(): return lax.all_to_all(pieces, RA, split_axis=0, concat_axis=0, tiled=True)]
    all_to_all x2 -> x3, starting transfers between devices: 10.7 us -> 18.8 us  [exchange(): return lax.all_to_all(pieces, RA, split_axis=0, concat_axis=0, tiled=True)]
    slice x0 -> x2, local copies, waits for them, and re-layouts: none -> 4.81 us  [the longest x1 3.58 us: shards(): second = in_parts(weights[:, :, later * rows:])]
    convert_element_type x2 -> x8, other arithmetic: 6.95 us -> 5.02 us  [in_parts(): part = weights[j * size:(j + 1) * size].astype(jnp.bfloat16)]
    unnamed x25 -> x37, local copies, waits for them, and re-layouts: 7.43 us -> 7.51 us
  transfers between devices with their start and end apart: 2 -> 3, of which waited for: 1 -> 2; matrix products, arithmetic and copies ran while one was open for 5% -> 6% of each run, Pallas kernels for 0% -> 0%
where the time goes in v3:
time: 177 us; the launch traced here: 176 us
  blocking collectives  98.9 us (56%)
  waiting for transfers between devices  27.9 us (16%)
  starting transfers between devices  18.8 us (11%)
  Pallas kernels  12.5 us (7%)
  local copies, waits for them, and re-layouts  12.3 us (7%)
  other arithmetic  5.07 us (3%)
    all_gather x1, blocking collectives, shards(): gathered = lax.all_gather(packed, CB, axis=0, tiled=True)  68.3 us
    all_to_all x2, blocking collectives, exchange(): return lax.all_to_all(pieces, RA, split_axis=0, concat_axis=0, tiled=True)  30.5 us
    all_to_all x3, waiting for transfers between devices, exchange(): return lax.all_to_all(pieces, RA, split_axis=0, concat_axis=0, tiled=True)  27.9 us
    all_to_all x3, starting transfers between devices, exchange(): return lax.all_to_all(pieces, RA, split_axis=0, concat_axis=0, tiled=True)  18.8 us
    unnamed x37, local copies, waits for them, and re-layouts  7.51 us
    pallas_call x2, Pallas kernels, block(): pl.pallas_call(functools.partial(block_body, start), out_shape=jax.ShapeD...  5.77 us
    convert_element_type x8, other arithmetic, in_parts(): part = weights[j * size:(j + 1) * size].astype(jnp.bfloat16)  5.02 us
    slice x1, local copies, waits for them, and re-layouts, shards(): second = in_parts(weights[:, :, later * rows:])  3.58 us
  transfers between devices with their start and end apart: 3, of which 2 were waited for; matrix products, arithmetic and copies ran while one was open for 6% of the time, Pallas kernels for 0%

profile of v3, /device:TPU:32, one launch (start us, length us, event | category | flops | bytes accessed | tf_op | source)
XLA Modules:
  0.0 175.9 jit_solution(7445871203640030293)
XLA Ops:
  0.0 2.7 %shard_map.154 = (bf16[1088,128]{1,0:T(8,128)(2,1)}, bf16[16,256,128]{2,1,0:T(8,128)(2,1)}) custom-call(f32[64,352]{1,0:T(8,128)} %refs_0_.1, f32[64,352]{1,0:T(8,128)} %refs_1_.1, f32[64,352]{1,0:T(8,128)} %bitcast.26, f32[64,352]{1,0:T(8,128)} %refs_3_.1, f32[64,352]{1,0:T(8,128)} %refs_4_.1, f32[64,352]{1,0:T(8,128)} %bitcast.27, bf16[256,128]{1,0:T(8,128)(2,1)} %refs_6_.1), custom_call_target="tpu_custom_call" | custom-call | tf_op jit(solution)/shard_map/pallas_call | solution.py:62
  2.7 0.0 copy-start.13
  2.7 7.2 %all-to-all-start = ((bf16[16,256,128]{2,1,0:T(8,128)(2,1)}), bf16[16,256,128]{2,1,0:T(8,128)(2,1)}, u32[]{:S(2)}, u32[]{:S(2)}) async-start(bf16[16,256,128]{2,1,0:T(8,128)(2,1)} %get-tuple-element.28), calls=%async_computation | async-start | bytes 2097152 | tf_op jit(solution)/shard_map/all_to_all | solution.py:225
  10.0 0.0 copy-done.13
  10.0 68.3 %all-gather.1 = f16[4456448]{0:T(1024)(128)(2,1)S(1)} all-gather(f16[139264]{0:T(1024)(128)(2,1)S(1)} %convert_bitcast_fusion), channel_id=1, replica_groups=mesh['ra_0'=4,'ra_1'=4,'cb_0'=16,'cb_1'=2] {'cb_0','cb_1'}, dimensions={0}, use_global_device_ids=true | all-gather | bytes 9191424 | tf_op jit(solution)/shard_map/all_gather | solution.py:265
  78.4 0.2 slice_convert_fusion.refs_0_
  78.6 1.2 slice.42
  79.8 2.0 %copy-done.12 = f16[4456448]{0:T(1024)(128)(2,1)} copy-done((f16[4456448]{0:T(1024)(128)(2,1)}, f16[4456448]{0:T(1024)(128)(2,1)S(1)}, u32[]{:S(2)}) %copy-start.12) | copy-done | bytes 8912920
  81.8 0.2 slice_convert_fusion.7.refs_1_
  82.1 0.2 slice_convert_fusion.6.refs_2_
  82.3 0.0 copy-start.14
  82.3 0.0 copy-start.15
  82.3 0.0 copy-start.7
  82.3 1.2 slice_convert_fusion.5.refs_3_
  83.5 0.0 copy-done.14
  83.5 0.0 copy-done.15
  83.5 0.0 all-to-all-done.pieces
  83.6 0.0 copy-done.7
  83.6 2.4 %shard_map.155 = (bf16[256,2048]{1,0:T(8,128)(2,1)S(1)}, f32[16,2048]{1,0:T(8,128)S(1)}) custom-call(bf16[16,256,128]{2,1,0:T(8,128)(2,1)} %all-to-all-done.pieces, f32[1,2048]{1,0:T(1,128)S(1)} %bitcast.16), custom_call_target="tpu_custom_call" | custom-call | tf_op jit(solution)/shard_map/pallas_call | solution.py:129
  85.9 0.0 copy-start.5
  85.9 0.7 copy-done.5
  86.6 1.3 copy-done
  87.9 2.3 %shard_map.156 = bf16[256,2048]{1,0:T(8,128)(2,1)S(1)} custom-call(bf16[256,2048]{1,0:T(8,128)(2,1)S(1)} %get-tuple-element.29.x, f32[1,352]{1,0:T(1,128)S(1)} %broadcast_in_dim.28.s_gate, f32[1,352]{1,0:T(1,128)S(1)} %broadcast_in_dim.29.s_up, bf16[4,2,576,128]{3,2,1,0:T(8,128)(2,1)S(1)} %slice_convert_fusion.refs_0_, ...), custom_call_target="tpu_custom_call" | custom-call | tf_op jit(solution)/shard_map/pallas_call | solution.py:187
  90.1 0.0 copy-start.2
  90.2 1.0 copy-done.2
  91.1 0.0 copy-start.9
  91.1 7.3 %all-to-all-start.1 = ((bf16[16,16,2048]{2,1,0:T(8,128)(2,1)}), bf16[16,16,2048]{2,1,0:T(8,128)(2,1)S(1)}, u32[]{:S(2)}, u32[]{:S(2)}) async-start(bf16[16,16,2048]{2,1,0:T(8,128)(2,1)} %bitcast.14), calls=%async_computation.1 | async-start | bytes 2097152 | tf_op jit(solution)/shard_map/all_to_all | solution.py:225
  98.4 18.2 %all-to-all-done.1.pieces = bf16[16,16,2048]{2,1,0:T(8,128)(2,1)S(1)} async-done(((bf16[16,16,2048]{2,1,0:T(8,128)(2,1)}), bf16[16,16,2048]{2,1,0:T(8,128)(2,1)S(1)}, u32[]{:S(2)}, u32[]{:S(2)}) %all-to-all-start.1) | async-done | bytes 1048608 | tf_op jit(solution)/shard_map/all_to_all | solution.py:225
  116.6 0.0 copy-done.9
  116.6 1.3 shard_map.157
  118.0 0.6 copy-done.3
  118.6 4.4 %all-to-all-start.2 = ((bf16[16,16,2048]{2,1,0:T(8,128)(2,1)}), bf16[16,16,2048]{2,1,0:T(8,128)(2,1)}, u32[]{:S(2)}, u32[]{:S(2)}) async-start(bf16[16,16,2048]{2,1,0:T(8,128)(2,1)} %get-tuple-element.39), calls=%async_computation.2 | async-start | bytes 2097152 | tf_op jit(solution)/shard_map/all_to_all | solution.py:225
  123.0 1.5 slice_convert_fusion.4.refs_0_
  124.5 3.6 %slice.37 = f16[16,2,576,128]{3,2,1,0:T(8,128)(2,1)S(1)} slice(f16[16,2,1088,128]{3,2,1,0:T(8,128)(2,1)} %bitcast.24), slice={[0:16], [0:2], [512:1088], [0:128]} | slice | bytes 9437184 | tf_op jit(solution)/shard_map/slice | solution.py:273
  128.0 0.2 slice_convert_fusion.3.refs_1_
  128.3 0.2 slice_convert_fusion.2.refs_2_
  128.5 1.3 slice_convert_fusion.1.refs_3_
  129.8 9.8 %all-to-all-done.2 = bf16[16,16,2048]{2,1,0:T(8,128)(2,1)} async-done(((bf16[16,16,2048]{2,1,0:T(8,128)(2,1)}), bf16[16,16,2048]{2,1,0:T(8,128)(2,1)}, u32[]{:S(2)}, u32[]{:S(2)}) %all-to-all-start.2) | async-done | bytes 1048608 | tf_op jit(solution)/shard_map/all_to_all | solution.py:225
  139.5 1.3 copy-done.1
  140.8 3.5 %shard_map.158 = bf16[256,2048]{1,0:T(8,128)(2,1)S(1)} custom-call(bf16[256,2048]{1,0:T(8,128)(2,1)} %bitcast.8.x, f32[1,352]{1,0:T(1,128)S(1)} %broadcast_in_dim.32.s_gate, f32[1,352]{1,0:T(1,128)S(1)} %broadcast_in_dim.33.s_up, bf16[4,2,576,128]{3,2,1,0:T(8,128)(2,1)S(1)} %slice_convert_fusion.4.refs_0_, ...), custom_call_target="tpu_custom_call" | custom-call | tf_op jit(solution)/shard_map/pallas_call | solution.py:187
  144.3 0.0 copy-start.10
  144.3 0.0 copy-start.11
  144.4 19.9 %all_to_all.25.pieces = bf16[16,16,2048]{2,1,0:T(8,128)(2,1)S(1)} all-to-all(bf16[16,16,2048]{2,1,0:T(8,128)(2,1)S(1)} %bitcast.15), channel_id=1, replica_groups=mesh['ra_0'=4,'ra_1'=4,'cb_0'=16,'cb_1'=2] {'ra_0','ra_1'}, dimensions={0} | all-to-all | bytes 2097152 | tf_op jit(solution)/shard_map/all_to_all | solution.py:225
  164.3 0.0 copy-done.4
  164.3 0.0 copy-done.11
  164.3 0.3 shard_map.159
  164.6 10.6 %all_to_all.26 = bf16[16,16,128]{2,1,0:T(8,128)(2,1)S(1)} all-to-all(bf16[16,16,128]{2,1,0:T(8,128)(2,1)S(1)} %shard_map.159), channel_id=1, replica_groups=mesh['ra_0'=4,'ra_1'=4,'cb_0'=16,'cb_1'=2] {'ra_0','ra_1'}, dimensions={0} | all-to-all | bytes 131072 | tf_op jit(solution)/shard_map/all_to_all | solution.py:225
  175.2 0.6 copy.18
  (19 shorter events, 0.1 us)
Async XLA Ops:
  2.7 7.2 %copy-start.13 = (bf16[1088,128]{1,0:T(8,128)(2,1)S(1)}, bf16[1088,128]{1,0:T(8,128)(2,1)}, u32[]{:S(2)}) copy-start(bf16[1088,128]{1,0:T(8,128)(2,1)} %get-tuple-element.27) | copy-start | bytes 835588
  2.7 80.8 %all-to-all-start = ((bf16[16,256,128]{2,1,0:T(8,128)(2,1)}), bf16[16,256,128]{2,1,0:T(8,128)(2,1)}, u32[]{:S(2)}, u32[]{:S(2)}) async-start(bf16[16,256,128]{2,1,0:T(8,128)(2,1)} %get-tuple-element.28), calls=%async_computation | async-start | bytes 2097152 | tf_op jit(solution)/shard_map/all_to_all | solution.py:225
  78.4 3.5 %copy-start.12 = (f16[4456448]{0:T(1024)(128)(2,1)}, f16[4456448]{0:T(1024)(128)(2,1)S(1)}, u32[]{:S(2)}) copy-start(f16[4456448]{0:T(1024)(128)(2,1)S(1)} %all-gather.1) | copy-start | bytes 26738692
  82.3 1.3 copy-start.14
  82.3 1.3 copy-start.15
  82.3 1.3 copy-start.7
  85.9 0.7 copy-start.5
  86.6 1.3 copy-start
  90.1 1.0 copy-start.2
  91.1 7.3 %copy-start.16 = (f32[352]{0:T(512)S(1)}, f32[352]{0:T(512)}, u32[]{:S(2)}) copy-start(f32[352]{0:T(512)} %param.26) | copy-start | bytes 4228
  91.1 7.3 %copy-start.17 = (f32[352]{0:T(512)S(1)}, f32[352]{0:T(512)}, u32[]{:S(2)}) copy-start(f32[352]{0:T(512)} %param.28) | copy-start | bytes 4228
  91.1 25.5 %copy-start.6 = (f32[16,2048]{1,0:T(8,128)S(1)}, f32[16,2048]{1,0:T(8,128)}, u32[]{:S(2)}) copy-start(f32[16,2048]{1,0:T(8,128)} %copy-done.5) | copy-start | bytes 393220
  91.1 25.5 %copy-start.8 = (f32[2048]{0:T(1024)S(1)}, f32[2048]{0:T(1024)}, u32[]{:S(2)}) copy-start(f32[2048]{0:T(1024)} %param.23) | copy-start | bytes 24580
  91.1 25.5 %copy-start.9 = (f32[2048]{0:T(1024)S(1)}, f32[2048]{0:T(1024)}, u32[]{:S(2)}) copy-start(f32[2048]{0:T(1024)} %param.24) | copy-start | bytes 24580
  91.1 25.5 %all-to-all-start.1 = ((bf16[16,16,2048]{2,1,0:T(8,128)(2,1)}), bf16[16,16,2048]{2,1,0:T(8,128)(2,1)S(1)}, u32[]{:S(2)}, u32[]{:S(2)}) async-start(bf16[16,16,2048]{2,1,0:T(8,128)(2,1)} %bitcast.14), calls=%async_computation.1 | async-start | bytes 2097152 | tf_op jit(solution)/shard_map/all_to_all | solution.py:225
  118.0 0.6 copy-start.3
  118.6 20.9 %all-to-all-start.2 = ((bf16[16,16,2048]{2,1,0:T(8,128)(2,1)}), bf16[16,16,2048]{2,1,0:T(8,128)(2,1)}, u32[]{:S(2)}, u32[]{:S(2)}) async-start(bf16[16,16,2048]{2,1,0:T(8,128)(2,1)} %get-tuple-element.39), calls=%async_computation.2 | async-start | bytes 2097152 | tf_op jit(solution)/shard_map/all_to_all | solution.py:225
  139.5 1.3 copy-start.1
  144.3 19.9 %copy-start.4 = (f32[16,2048]{1,0:T(8,128)S(1)}, f32[16,2048]{1,0:T(8,128)}, u32[]{:S(2)}) copy-start(f32[16,2048]{1,0:T(8,128)} %copy-done.3) | copy-start | bytes 393220
  144.3 19.9 %copy-start.10 = (f32[2048]{0:T(1024)S(1)}, f32[2048]{0:T(1024)}, u32[]{:S(2)}) copy-start(f32[2048]{0:T(1024)} %param.30) | copy-start | bytes 24580
  144.3 19.9 %copy-start.11 = (f32[2048]{0:T(1024)S(1)}, f32[2048]{0:T(1024)}, u32[]{:S(2)}) copy-start(f32[2048]{0:T(1024)} %param.31) | copy-start | bytes 24580

commit v4 on v2

--- a/solution.py
+++ b/solution.py
@@ -17,6 +17,7 @@
 TILES = 17
 PART = 9
 WIDE = 4 * TILE
+CUT = 4
 EPS = 1e-06
 LIFT = 2.0**18
 ROOM = pltpu.CompilerParams(vmem_limit_bytes=20 * 1024 * 1024)
@@ -147,9 +148,11 @@
 
 def block_body(start, x, s_gate, s_up, *refs):
     parts, (out, scales) = refs[:-2], refs[-2:]
-    share = HALF // len(parts)
+    ends = [0]
+    for part in parts:
+        ends.append(ends[-1] + part.shape[0] * part.shape[2] // PART)
     places = [
-        (part, side, slice(side * HALF + p * share, side * HALF + (p + 1) * share))
+        (part, side, slice(side * HALF + ends[p], side * HALF + ends[p + 1]))
         for p, part in enumerate(parts)
         for side in (0, 1)
     ]
@@ -229,7 +232,7 @@
 
 
 def in_parts(weights):
-    return [part.astype(jnp.bfloat16) for part in jnp.split(weights, 2, axis=0)]
+    return [part.astype(jnp.bfloat16) for part in jnp.split(weights, [CUT], axis=0)]
 
 
 def shards(

time: 172 us -> 174 us (1.012)
  Pallas kernels: 10 us -> 12.5 us
    unnamed x25 -> x29, local copies, waits for them, and re-layouts: 7.43 us -> 6.23 us
    convert_element_type x2 -> x4, other arithmetic: 6.95 us -> 7.37 us  [in_parts(): part.astype(jnp.bfloat16)]
where the time goes in v4:
time: 174 us; the launch traced here: 173 us
  blocking collectives  123 us (71%)
  Pallas kernels  12.5 us (7%)
  waiting for transfers between devices  11.6 us (7%)
  starting transfers between devices  11.4 us (7%)
  other arithmetic  8.38 us (5%)
  local copies, waits for them, and re-layouts  6.25 us (4%)
    all_gather x1, blocking collectives, shards(): gathered = lax.all_gather(packed, CB, axis=0, tiled=True)  68 us
    all_to_all x3, blocking collectives, exchange(): return lax.all_to_all(pieces, RA, split_axis=0, concat_axis=0, tiled=True)  54.9 us
    all_to_all x2, waiting for transfers between devices, exchange(): return lax.all_to_all(pieces, RA, split_axis=0, concat_axis=0, tiled=True)  11.6 us
    all_to_all x2, starting transfers between devices, exchange(): return lax.all_to_all(pieces, RA, split_axis=0, concat_axis=0, tiled=True)  11.4 us
    convert_element_type x4, other arithmetic, in_parts(): part.astype(jnp.bfloat16)  7.37 us
    unnamed x29, local copies, waits for them, and re-layouts  6.23 us
    pallas_call x2, Pallas kernels, block(): pl.pallas_call(functools.partial(block_body, start), out_shape=jax.ShapeD...  5.78 us
  transfers between devices with their start and end apart: 2, of which 1 were waited for; matrix products, arithmetic and copies ran while one was open for 5% of the time, Pallas kernels for 0%

profile of v4, /device:TPU:32, one launch (start us, length us, event | category | flops | bytes accessed | tf_op | source)
XLA Modules:
  0.0 173.4 jit_solution(2971355525384017939)
XLA Ops:
  0.0 2.7 %shard_map.154 = (bf16[1088,128]{1,0:T(8,128)(2,1)}, bf16[16,256,128]{2,1,0:T(8,128)(2,1)}) custom-call(f32[64,352]{1,0:T(8,128)} %refs_0_.1, f32[64,352]{1,0:T(8,128)} %refs_1_.1, f32[64,352]{1,0:T(8,128)} %bitcast.26, f32[64,352]{1,0:T(8,128)} %refs_3_.1, f32[64,352]{1,0:T(8,128)} %refs_4_.1, f32[64,352]{1,0:T(8,128)} %bitcast.27, bf16[256,128]{1,0:T(8,128)(2,1)} %refs_6_.1), custom_call_target="tpu_custom_call" | custom-call | tf_op jit(solution)/shard_map/pallas_call | solution.py:62
  2.7 7.1 %all-to-all-start = ((bf16[16,256,128]{2,1,0:T(8,128)(2,1)}), bf16[16,256,128]{2,1,0:T(8,128)(2,1)}, u32[]{:S(2)}, u32[]{:S(2)}) async-start(bf16[16,256,128]{2,1,0:T(8,128)(2,1)} %get-tuple-element.14), calls=%async_computation | async-start | bytes 2097152 | tf_op jit(solution)/shard_map/all_to_all | solution.py:227
  9.8 1.0 convert_bitcast_fusion
  10.8 0.0 copy-start.10
  10.8 0.0 copy-start.11
  10.9 68.0 %all-gather.1 = f16[4456448]{0:T(1024)(128)(2,1)S(1)} all-gather(f16[139264]{0:T(1024)(128)(2,1)S(1)} %convert_bitcast_fusion), channel_id=1, replica_groups=mesh['ra_0'=4,'ra_1'=4,'cb_0'=16,'cb_1'=2] {'cb_0','cb_1'}, dimensions={0}, use_global_device_ids=true | all-gather | bytes 9191424 | tf_op jit(solution)/shard_map/all_gather | solution.py:261
  78.9 0.0 copy-done.10
  78.9 0.0 copy-start.9
  78.9 0.0 copy-done.11
  78.9 1.4 slice_convert_fusion.2.refs_0_
  80.3 2.4 %copy-done.9 = f16[4456448]{0:T(1024)(128)(2,1)} copy-done((f16[4456448]{0:T(1024)(128)(2,1)}, f16[4456448]{0:T(1024)(128)(2,1)S(1)}, u32[]{:S(2)}) %copy-start.9) | copy-done | bytes 8912920
  82.7 0.0 copy-start.4
  82.7 0.7 slice_convert_fusion.refs_1_
  83.5 0.0 all-to-all-done.pieces
  83.5 0.0 copy-done.4
  83.5 2.4 %shard_map.155 = (bf16[256,2048]{1,0:T(8,128)(2,1)S(1)}, f32[16,2048]{1,0:T(8,128)S(1)}) custom-call(bf16[16,256,128]{2,1,0:T(8,128)(2,1)} %all-to-all-done.pieces, f32[1,2048]{1,0:T(1,128)S(1)} %bitcast.16), custom_call_target="tpu_custom_call" | custom-call | tf_op jit(solution)/shard_map/pallas_call | solution.py:129
  85.8 0.0 copy-start
  85.9 1.3 copy-done
  87.1 0.0 copy-start.5
  87.1 0.0 copy-start.6
  87.1 2.3 %shard_map.156 = bf16[256,2048]{1,0:T(8,128)(2,1)S(1)} custom-call(bf16[256,2048]{1,0:T(8,128)(2,1)S(1)} %get-tuple-element.15.x, f32[1,352]{1,0:T(1,128)S(1)} %broadcast_in_dim.28.s_gate, f32[1,352]{1,0:T(1,128)S(1)} %broadcast_in_dim.29.s_up, bf16[4,2,576,128]{3,2,1,0:T(8,128)(2,1)S(1)} %copy-done, bf16[12,2,576,128]{3,2,1,0:T(8,128)(2,1)S(1)} %slice_convert_fusion.refs_1_), custom_call_target="tpu_custom_call" | custom-call | tf_op jit(solution)/shard_map/pallas_call | solution.py:189
  89.4 0.0 copy-start.12
  89.4 0.0 copy-start.13
  89.4 25.0 %all_to_all.25.pieces = bf16[16,16,2048]{2,1,0:T(8,128)(2,1)S(1)} all-to-all(bf16[16,16,2048]{2,1,0:T(8,128)(2,1)S(1)} %bitcast.14), channel_id=1, replica_groups=mesh['ra_0'=4,'ra_1'=4,'cb_0'=16,'cb_1'=2] {'ra_0','ra_1'}, dimensions={0} | all-to-all | bytes 2097152 | tf_op jit(solution)/shard_map/all_to_all | solution.py:227
  114.4 0.0 copy-done.5
  114.4 0.0 copy-done.6
  114.4 1.3 shard_map.157
  115.7 0.0 copy-start.2
  115.7 0.6 copy-done.2
  116.3 4.3 %all-to-all-start.2 = ((bf16[16,16,2048]{2,1,0:T(8,128)(2,1)}), bf16[16,16,2048]{2,1,0:T(8,128)(2,1)}, u32[]{:S(2)}, u32[]{:S(2)}) async-start(bf16[16,16,2048]{2,1,0:T(8,128)(2,1)} %get-tuple-element.18), calls=%async_computation.2 | async-start | bytes 2097152 | tf_op jit(solution)/shard_map/all_to_all | solution.py:227
  120.7 0.0 copy-done.12
  120.7 0.0 copy-done.13
  120.7 2.5 %slice_convert_fusion.3.refs_0_ = bf16[4,2,576,128]{3,2,1,0:T(8,128)(2,1)} fusion(f16[16,2,1088,128]{3,2,1,0:T(8,128)(2,1)} %bitcast.23), kind=kLoop, calls=%fused_computation.3 | loop fusion | flops 589824 | bytes 2359296 | tf_op jit(solution)/shard_map/convert_element_type | solution.py:235
  123.2 2.7 %slice_convert_fusion.1.refs_1_ = bf16[12,2,576,128]{3,2,1,0:T(8,128)(2,1)S(1)} fusion(f16[16,2,1088,128]{3,2,1,0:T(8,128)(2,1)} %bitcast.24), kind=kLoop, calls=%fused_computation.1 | loop fusion | flops 1769472 | bytes 7077888 | tf_op jit(solution)/shard_map/convert_element_type | solution.py:235
  126.0 11.6 %all-to-all-done.2 = bf16[16,16,2048]{2,1,0:T(8,128)(2,1)} async-done(((bf16[16,16,2048]{2,1,0:T(8,128)(2,1)}), bf16[16,16,2048]{2,1,0:T(8,128)(2,1)}, u32[]{:S(2)}, u32[]{:S(2)}) %all-to-all-start.2) | async-done | bytes 1048608 | tf_op jit(solution)/shard_map/all_to_all | solution.py:227
  137.6 0.0 copy-start.1
  137.6 1.3 copy-done.1
  138.9 0.0 copy-start.3
  138.9 0.0 copy-start.7
  138.9 0.0 copy-start.8
  138.9 3.5 %shard_map.158 = bf16[256,2048]{1,0:T(8,128)(2,1)S(1)} custom-call(bf16[256,2048]{1,0:T(8,128)(2,1)} %bitcast.8.x, f32[1,352]{1,0:T(1,128)S(1)} %broadcast_in_dim.32.s_gate, f32[1,352]{1,0:T(1,128)S(1)} %broadcast_in_dim.33.s_up, bf16[4,2,576,128]{3,2,1,0:T(8,128)(2,1)S(1)} %copy-done.1, bf16[12,2,576,128]{3,2,1,0:T(8,128)(2,1)S(1)} %slice_convert_fusion.1.refs_1_), custom_call_target="tpu_custom_call" | custom-call | tf_op jit(solution)/shard_map/pallas_call | solution.py:189
  142.4 19.4 %all_to_all.26.pieces = bf16[16,16,2048]{2,1,0:T(8,128)(2,1)S(1)} all-to-all(bf16[16,16,2048]{2,1,0:T(8,128)(2,1)S(1)} %bitcast.15), channel_id=1, replica_groups=mesh['ra_0'=4,'ra_1'=4,'cb_0'=16,'cb_1'=2] {'ra_0','ra_1'}, dimensions={0} | all-to-all | bytes 2097152 | tf_op jit(solution)/shard_map/all_to_all | solution.py:227
  161.8 0.0 copy-done.3
  161.8 0.0 copy-done.7
  161.8 0.0 copy-done.8
  161.8 0.3 shard_map.159
  162.1 10.6 %all_to_all.27 = bf16[16,16,128]{2,1,0:T(8,128)(2,1)S(1)} all-to-all(bf16[16,16,128]{2,1,0:T(8,128)(2,1)S(1)} %shard_map.159), channel_id=1, replica_groups=mesh['ra_0'=4,'ra_1'=4,'cb_0'=16,'cb_1'=2] {'ra_0','ra_1'}, dimensions={0} | all-to-all | bytes 131072 | tf_op jit(solution)/shard_map/all_to_all | solution.py:227
  172.7 0.6 copy.18
  (4 shorter events, 0.0 us)
Async XLA Ops:
  2.7 80.7 %all-to-all-start = ((bf16[16,256,128]{2,1,0:T(8,128)(2,1)}), bf16[16,256,128]{2,1,0:T(8,128)(2,1)}, u32[]{:S(2)}, u32[]{:S(2)}) async-start(bf16[16,256,128]{2,1,0:T(8,128)(2,1)} %get-tuple-element.14), calls=%async_computation | async-start | bytes 2097152 | tf_op jit(solution)/shard_map/all_to_all | solution.py:227
  10.8 68.1 %copy-start.10 = (f32[352]{0:T(512)S(1)}, f32[352]{0:T(512)}, u32[]{:S(2)}) copy-start(f32[352]{0:T(512)} %param.19) | copy-start | bytes 4228
  10.8 68.1 %copy-start.11 = (f32[352]{0:T(512)S(1)}, f32[352]{0:T(512)}, u32[]{:S(2)}) copy-start(f32[352]{0:T(512)} %param.21) | copy-start | bytes 4228
  78.9 3.8 %copy-start.9 = (f16[4456448]{0:T(1024)(128)(2,1)}, f16[4456448]{0:T(1024)(128)(2,1)S(1)}, u32[]{:S(2)}) copy-start(f16[4456448]{0:T(1024)(128)(2,1)S(1)} %all-gather.1) | copy-start | bytes 26738692
  82.7 0.8 copy-start.4
  85.8 1.3 copy-start
  87.1 27.3 %copy-start.5 = (f32[2048]{0:T(1024)S(1)}, f32[2048]{0:T(1024)}, u32[]{:S(2)}) copy-start(f32[2048]{0:T(1024)} %param.23) | copy-start | bytes 24580
  87.1 27.3 %copy-start.6 = (f32[2048]{0:T(1024)S(1)}, f32[2048]{0:T(1024)}, u32[]{:S(2)}) copy-start(f32[2048]{0:T(1024)} %param.24) | copy-start | bytes 24580
  89.4 31.3 %copy-start.12 = (f32[352]{0:T(512)S(1)}, f32[352]{0:T(512)}, u32[]{:S(2)}) copy-start(f32[352]{0:T(512)} %param.26) | copy-start | bytes 4228
  89.4 31.3 %copy-start.13 = (f32[352]{0:T(512)S(1)}, f32[352]{0:T(512)}, u32[]{:S(2)}) copy-start(f32[352]{0:T(512)} %param.28) | copy-start | bytes 4228
  115.7 0.7 copy-start.2
  116.3 21.2 %all-to-all-start.2 = ((bf16[16,16,2048]{2,1,0:T(8,128)(2,1)}), bf16[16,16,2048]{2,1,0:T(8,128)(2,1)}, u32[]{:S(2)}, u32[]{:S(2)}) async-start(bf16[16,16,2048]{2,1,0:T(8,128)(2,1)} %get-tuple-element.18), calls=%async_computation.2 | async-start | bytes 2097152 | tf_op jit(solution)/shard_map/all_to_all | solution.py:227
  137.6 1.3 copy-start.1
  138.9 22.9 %copy-start.3 = (f32[16,2048]{1,0:T(8,128)S(1)}, f32[16,2048]{1,0:T(8,128)}, u32[]{:S(2)}) copy-start(f32[16,2048]{1,0:T(8,128)} %copy-done.2) | copy-start | bytes 393220
  138.9 22.9 %copy-start.7 = (f32[2048]{0:T(1024)S(1)}, f32[2048]{0:T(1024)}, u32[]{:S(2)}) copy-start(f32[2048]{0:T(1024)} %param.30) | copy-start | bytes 24580
  138.9 22.9 %copy-start.8 = (f32[2048]{0:T(1024)S(1)}, f32[2048]{0:T(1024)}, u32[]{:S(2)}) copy-start(f32[2048]{0:T(1024)} %param.31) | copy-start | bytes 24580
